TPU v7x, 512 devices: a whole 4x8x8 slice. The times are simulated.
512 devices in a mesh: sp: 64 (over z, y), fs: 4 (over x), tp: 2 (over core).
Axes of the slice: x: 4, y: 8, z: 8, core: 2. Of those that a mesh axis runs over, the one named last changes fastest.
Arguments:
- tokens: bfloat16 [131072, 2048], P(('fs', 'sp', 'tp')), parts along dimension 0, may hold values from -60 to 60
- norm_gain: float32 [2048], replicated, may hold values from 0.1 to 1.9
- pool_in: bfloat16 [2048, 512], P('sp', 'tp'), may hold values from -0.125 to 0.125
- gate_in: bfloat16 [2048, 1024], P('sp', 'tp'), may hold values from -0.125 to 0.125
- value_in: bfloat16 [2048, 1024], P('sp', 'tp'), may hold values from -0.125 to 0.125
- pool_mix: bfloat16 [4, 128, 128], P('tp'), may hold values from -0.5 to 0.5
- averaging_factor: float32 [512], P('tp'), may hold values from 0.25 to 0.75
- conv_taps: float32 [4, 1024], P(None, 'tp'), may hold values from -3 to 3
- rate_mix: bfloat16 [16, 64, 64], P('tp'), may hold values from -0.75 to 0.75
- input_mix: bfloat16 [16, 64, 64], P('tp'), may hold values from -0.75 to 0.75
- log_rate: float32 [1024], P('tp'), may hold values from 1.5 to 16
- decay_shift: float32 [64, 32768], P(('fs', 'tp'), 'sp'), parts along dimension 0, may hold values from -1.1 to 0
- initial_state: float32 [4096], P(('fs', 'tp')), parts along dimension 0, may hold values from -6 to 6
- out_pool: bfloat16 [2048, 512], P('sp', 'tp'), may hold values from -0.15625 to 0.15625
- out_rnn: bfloat16 [2048, 1024], P('sp', 'tp'), may hold values from -0.15625 to 0.15625
Outputs:
- mixed: bfloat16 [131072, 2048], P(('fs', 'sp', 'tp')), parts along dimension 0
There are 4 independent parts, one for each index of `fs`. A program takes and returns all parts, laid end to end along the dimension named above; an argument that names none is the same for every part. Nothing has to cross between parts.
All inputs are finite; a program needn't handle non-finite values.
Results may differ from a plain program's by a relative error of at most 0.012.
Values may be sent and summed in bfloat16 or wider, within the bound.
A program may use at most 64 MiB of HBM per device.

v0:
```python
import jax
import jax.numpy as jnp
from jax import lax
from jax.sharding import PartitionSpec as P

GROUP_WIDTH = 128
HEAD_DIM = 64
TAPS = 4
REACH = 16


epsilon = 1e-06
sharpness = 8.0


def sent_together(arrays, axis, dim, along):
    widths = [a.shape[along] for a in arrays]
    both = jnp.concatenate(arrays, axis=along)
    result = lax.all_gather(both, axis, axis=dim, tiled=True)
    return tuple(jnp.split(result, [sum(widths[:k]) for k in range(1, len(widths))], axis=along))


def from_everyone(array, axis):
    count = lax.axis_size(axis)
    return lax.all_to_all(
        jnp.broadcast_to(array[None], (count, *array.shape)), axis, 0, 0, tiled=True
    )


def joined_along(parts, dim):
    dims = list(parts.shape[1:])
    dims[dim] *= parts.shape[0]
    return jnp.moveaxis(parts, 0, dim).reshape(dims)


def collect(array, axis, dim):
    parts = from_everyone(array, axis)
    return joined_along(parts, dim)


def from_behind(value, axis, steps):
    count = lax.axis_size(axis)
    first, last = (max(0, -steps), min(count, count - steps))
    return lax.ppermute(value, axis, [(source, source + steps) for source in range(first, last)])


def gathered_once(array, axis):
    leaves = jax.tree.leaves(array)
    sequence = sorted(range(len(leaves)), key=lambda k: -leaves[k].size)
    width = (1, *leaves[sequence[0]].shape)[-1]
    lines = [
        jnp.pad(leaves[k].reshape(-1), (0, -leaves[k].size % width)).reshape(-1, width)
        for k in sequence
    ]
    both, at, found = (from_everyone(jnp.concatenate(lines), axis), 0, {})
    for k, line in zip(sequence, lines):
        slab = both[:, at : at + len(line)].reshape(len(both), -1)
        found[k] = slab[:, : leaves[k].size].reshape(-1, *leaves[k].shape)
        at += len(line)
    numbers = iter(range(len(leaves)))
    return jax.tree.map(lambda _: found[next(numbers)], array)


def folded_in_pairs(pieces, combine):
    while len(jax.tree.leaves(pieces)[0]) > 1:
        pieces = jax.vmap(combine)(
            *(jax.tree.map(lambda part: part[side::2], pieces) for side in (0, 1))
        )
    return jax.tree.map(lambda part: part[0], pieces)


def entering(array, axis, combine, identity):
    count, index = (lax.axis_size(axis), lax.axis_index(axis))
    passed = jnp.arange(count) < index

    def kept(part, zero, own):
        part = jnp.where(
            passed.reshape(-1, *(1 for _ in own.shape)), part, jnp.asarray(zero, own.dtype)
        )
        return part

    pieces = gathered_once(array, axis)
    return folded_in_pairs(jax.tree.map(kept, pieces, identity, array), combine)


def cut_along(array, dim, count):
    dims = array.shape
    parts = array.reshape(*dims[:dim], count, dims[dim] // count, *dims[dim + 1 :])
    return jnp.moveaxis(parts, dim, 0)


def sent_and_summed(array, axis, dim):
    parts = cut_along(array, dim, lax.axis_size(axis))
    arrived = lax.all_to_all(parts, axis, split_axis=0, concat_axis=0, tiled=True)
    return arrived.sum(axis=0)


def chain_pairs(first_pair, second_pair):
    return (first_pair[0] * second_pair[0], second_pair[0] * first_pair[1] + second_pair[1])


def right_product(left_rows, weight_rows):
    return lax.dot_general(
        left_rows, weight_rows, (((1,), (1,)), ((), ())), preferred_element_type=jnp.float32
    )


def shards(
    tokens,
    norm_gain,
    pool_in,
    gate_in,
    value_in,
    pool_mix,
    averaging_factor,
    conv_taps,
    rate_mix,
    input_mix,
    log_rate,
    decay_shift,
    initial_state,
    out_pool,
    out_rnn,
):
    tp_index = lax.axis_index("tp")
    sp_index = lax.axis_index("sp")
    gathered = sent_together((pool_in, gate_in, value_in, out_pool, out_rnn), "sp", 0, 1)
    pool_weight, gate_weight, value_weight, averaging_exit_matrix, out_rnn_weight = gathered
    pool_width = pool_weight.shape[1]
    rnn_width = gate_weight.shape[1]
    widened = collect(tokens, "tp", 0).astype(jnp.float32)
    scaling = lax.rsqrt(jnp.mean(widened * widened, axis=1, keepdims=True) + epsilon)
    normed = (widened * scaling * norm_gain[None, :]).astype(jnp.bfloat16)
    outputs = [
        jnp.dot(normed, matrix, preferred_element_type=jnp.float32).astype(jnp.bfloat16)
        for matrix in (pool_weight, gate_weight, value_weight)
    ]
    projected = jnp.concatenate(outputs, axis=1)
    block_rows = projected.shape[0]
    pool_pre = projected[:, :pool_width]
    gate_pre = projected[:, pool_width : pool_width + rnn_width]
    value_pre = projected[:, pool_width + rnn_width :]
    edge_rows = jnp.concatenate(
        [pool_pre[block_rows - REACH :], value_pre[block_rows - REACH :]], axis=1
    )
    earlier_rows = from_behind(edge_rows, "sp", 1)
    pool_values = pool_pre.astype(jnp.float32)
    pool_padded = jnp.concatenate([earlier_rows[:, :pool_width], pool_pre], axis=0).astype(
        jnp.float32
    )
    value_padded = jnp.concatenate([earlier_rows[:, pool_width:], value_pre], axis=0).astype(
        jnp.float32
    )
    groups_here = pool_width // GROUP_WIDTH
    group_index = tp_index * groups_here + jnp.arange(pool_width, dtype=jnp.int32) // GROUP_WIDTH
    window = jnp.left_shift(jnp.int32(2), group_index)
    positions = sp_index * block_rows + jnp.arange(block_rows, dtype=jnp.int32)
    window_sum = jnp.zeros((block_rows, pool_width), jnp.float32)
    for steps_back in range(REACH):
        lagged = pool_padded[REACH - steps_back : REACH - steps_back + block_rows]
        window_sum = window_sum + jnp.where(steps_back < window[None, :], lagged, 0.0)
    counts = jnp.minimum(positions[:, None] + 1, window[None, :]).astype(jnp.float32)
    pooled = (window_sum / counts - pool_values).astype(jnp.bfloat16)
    grouped = pooled.reshape(block_rows, groups_here, GROUP_WIDTH)
    mixed_groups = jnp.einsum("tgc,gcd->tgd", grouped, pool_mix, preferred_element_type=jnp.float32)
    pool_out = (mixed_groups.reshape(block_rows, pool_width) * averaging_factor[None, :]).astype(
        jnp.bfloat16
    )
    start_row = REACH - TAPS + 1
    convolved = conv_taps[0][None, :] * value_padded[start_row : start_row + block_rows]
    for tap_index in range(1, TAPS):
        convolved = (
            convolved
            + conv_taps[tap_index][None, :]
            * value_padded[start_row + tap_index : start_row + tap_index + block_rows]
        )
    conv_out = convolved.astype(jnp.bfloat16)
    heads_here = rnn_width // HEAD_DIM
    both_mixes = jnp.concatenate([rate_mix, input_mix], axis=2)
    gate_terms = jnp.einsum(
        "thc,hcd->thd",
        conv_out.reshape(block_rows, heads_here, HEAD_DIM),
        both_mixes,
        preferred_element_type=jnp.float32,
    )
    rate_gate = jax.nn.sigmoid(gate_terms[:, :, :HEAD_DIM]).reshape(block_rows, rnn_width)
    input_gate = jax.nn.sigmoid(gate_terms[:, :, HEAD_DIM:]).reshape(block_rows, rnn_width)
    shifts = jnp.broadcast_to(
        jnp.transpose(decay_shift)[:, :, None], (block_rows, heads_here, HEAD_DIM)
    ).reshape(block_rows, rnn_width)
    log_decay = -sharpness * rate_gate * jax.nn.softplus(-log_rate)[None, :] + shifts
    decays = jnp.exp(log_decay)
    drives = jnp.sqrt(-jnp.expm1(2.0 * log_decay)) * input_gate * conv_out.astype(jnp.float32)
    cumulative, local_state = lax.associative_scan(chain_pairs, (decays, drives), axis=0)
    identity = (jnp.ones((rnn_width,), jnp.float32), jnp.zeros((rnn_width,), jnp.float32))
    prior_decay, prior_state = entering(
        (cumulative[block_rows - 1], local_state[block_rows - 1]), "sp", chain_pairs, identity
    )
    carried = prior_decay * initial_state + prior_state
    hidden_state = local_state + cumulative * carried[None, :]
    rnn_out = (jax.nn.gelu(gate_pre.astype(jnp.float32), approximate=True) * hidden_state).astype(
        jnp.bfloat16
    )
    return sent_and_summed(
        right_product(pool_out, averaging_exit_matrix) + right_product(rnn_out, out_rnn_weight),
        "tp",
        0,
    ).astype(jnp.bfloat16)


def solution(mesh):
    placed = (
        P(("fs", "sp", "tp"), None),
        P(),
        P("sp", "tp"),
        P("sp", "tp"),
        P("sp", "tp"),
        P("tp", None, None),
        P("tp"),
        P(None, "tp"),
        P("tp", None, None),
        P("tp", None, None),
        P("tp"),
        P(("fs", "tp"), "sp"),
        P(("fs", "tp")),
        P("sp", "tp"),
        P("sp", "tp"),
    )
    return jax.shard_map(
        shards, mesh=mesh, in_specs=placed, out_specs=P(("fs", "sp", "tp"), None), check_vma=False
    )
```

profile of v0, /device:TPU:1, one launch (start us, length us, event | category | flops | bytes accessed | tf_op | source)
XLA Modules:
  0.0 271.6 jit_solution(7703874203059547549)
XLA Ops:
  11.0 2.8 %broadcast_in_dim.164 = bf16[2,256,2048]{2,1,0:T(8,128)(2,1)} broadcast(bf16[256,2048]{1,0:T(8,128)(2,1)} %param.15), dimensions={1,2} | broadcast | bytes 3145728 | tf_op jit(solution)/shard_map/broadcast_in_dim | solution.py:26
  13.8 10.6 %all-to-all-start = ((bf16[2,256,2048]{2,1,0:T(8,128)(2,1)}), bf16[2,256,2048]{2,1,0:T(8,128)(2,1)S(1)}, u32[]{:S(2)}, u32[]{:S(2)}) async-start(bf16[2,256,2048]{2,1,0:T(8,128)(2,1)} %broadcast_in_dim.164), calls=%async_computation | async-start | bytes 4194304 | tf_op jit(solution)/shard_map/all_to_all | solution.py:25
  24.4 2.5 all-to-all-done
  33.1 1.9 fusion.1
  34.9 80.5 %all-gather.2.cloned.1.call-done = bf16[2048,2048]{1,0:T(8,128)(2,1)} async-done(((bf16[32,2048]{1,0:T(8,128)(2,1)}), bf16[2048,2048]{1,0:T(8,128)(2,1)}) %all-gather.2.cloned.1.call-update) | async-done | bytes 8388624 | tf_op jit(solution)/shard_map/all_gather | solution.py:19
  115.4 2.6 convolution_convert_fusion
  118.7 2.8 %fusion.7 = bf16[512,512]{1,0:T(8,128)(2,1)S(1)} fusion(bf16[512,2048]{1,0:T(8,128)(2,1)S(1)} %copy-done.1, bf16[2048,2048]{1,0:T(8,128)(2,1)} %all-gather.2.cloned.1.call-done), kind=kOutput, calls=%fused_computation.15 | convolution fusion | flops 1074003968 | bytes 4718592 | tf_op jit(solution)/shard_map/dot_general | solution.py:135
  121.6 3.3 %collective-permute-start = (bf16[16,768]{1,0:T(8,128)(2,1)S(1)}, bf16[16,768]{1,0:T(8,128)(2,1)S(1)}, u32[]{:S(2)}, u32[]{:S(2)}) collective-permute-start(bf16[16,768]{1,0:T(8,128)(2,1)S(1)} %pad_maximum_fusion.10), channel_id=1, source_target_pairs={{0,8},{8,16},{16,24},{24,32},{32,40},{40,48},{48,56},{56,64},{64,7... | collective-permute-start | bytes 73736 | tf_op jit(solution)/shard_map/ppermute | solution.py:44
  125.6 1.3 copy.39
  126.9 1.2 maximum_convert_fusion
  128.1 1.3 fusion.33
  129.3 2.1 copy.37
  131.4 1.6 convolution_bitcast_fusion
  133.0 1.9 fusion.28
  134.9 2.6 copy.40
  137.5 2.5 copy.38
  140.0 4.0 %convert_multiply_fusion.3 = (f32[512,512]{1,0:T(8,128)S(1)}, f32[512,512]{1,0:T(8,128)}) fusion(f32[512,512]{1,0:T(8,128)} %copy.40, f32[512,512]{1,0:T(8,128)} %copy.39, f32[512,512]{1,0:T(8,128)} %copy.38, f32[512]{0:T(512)S(1)} %fusion.85, f32[528,512]{1,0:T(8,128)S(1)} %maximum_convert_fusion, f32[512]{0:T(512)S(1)} %bitcast.58, f32[512]{0:T(512)S(1)} %bitcast.60, ...), kind=kLoop, calls=%fused_computation.44 | loop fusion | flops 3932160 | bytes 9447424 | tf_op jit(solution)/shard_map/mul | solution.py:193
  145.0 3.7 %slice.534 = f32[255,512]{1,0:T(8,128)} slice(f32[512,512]{1,0:T(8,128)} %copy-done.3), slice={[2:512:2], [0:512:1]} | slice | bytes 1044480 | tf_op jit(solution)/shard_map/slice | solution.py:194
  148.7 3.6 %slice.472 = f32[256,512]{1,0:T(8,128)} slice(f32[512,512]{1,0:T(8,128)} %copy-done.3), slice={[1:512:2], [0:512:1]} | slice | bytes 1048576 | tf_op jit(solution)/shard_map/slice | solution.py:194
  152.4 3.6 %slice.471 = f32[256,512]{1,0:T(8,128)} slice(f32[512,512]{1,0:T(8,128)} %copy-done.3), slice={[0:511:2], [0:512:1]} | slice | bytes 1048576 | tf_op jit(solution)/shard_map/slice | solution.py:194
  156.0 2.1 slice.474
  158.1 2.1 slice.470
  160.1 2.1 slice.469
  162.2 1.7 multiply_add_fusion.1
  164.0 1.4 slice.532
  165.7 1.4 slice.477
  167.7 1.4 slice.475
  169.1 1.0 multiply_add_fusion.2
  172.0 1.8 maximum_convert_fusion.1
  175.7 1.9 fusion.70
  177.7 1.7 pad_maximum_fusion.2
  179.3 1.1 pad.124
  180.4 2.6 pad.125
  183.0 1.7 pad.143
  184.7 2.1 add.490
  186.8 1.9 add.480
  188.7 1.2 fusion.41
  190.8 2.1 pad.144
  192.9 1.9 pad_maximum_fusion
  194.8 4.6 %pad.126 = f32[512,512]{1,0:T(8,128)} pad(f32[256,512]{1,0:T(8,128)} %pad_maximum_fusion, f32[]{:T(128)} %constant.95.clone.1), padding=0_1_1x0_0_0 | pad | bytes 1572868 | tf_op jit(solution)/shard_map/pad | solution.py:194
  199.5 4.6 %pad.127 = f32[512,512]{1,0:T(8,128)} pad(f32[256,512]{1,0:T(8,128)} %add.480, f32[]{:T(128)} %constant.95.clone.1), padding=1_0_1x0_0_0 | pad | bytes 1572868 | tf_op jit(solution)/shard_map/pad | solution.py:194
  204.2 4.6 %pad.145 = f32[512,512]{1,0:T(8,128)} pad(f32[256,512]{1,0:T(8,128)} %add.490, f32[]{:T(128)} %constant.95.clone.1), padding=1_0_1x0_0_0 | pad | bytes 1572868 | tf_op jit(solution)/shard_map/pad | solution.py:194
  211.0 10.5 %all-to-all-start.1 = ((f32[64,2,512]{2,1,0:T(2,128)}), f32[64,2,512]{2,1,0:T(2,128)S(1)}, u32[]{:S(2)}, u32[]{:S(2)}) async-start(f32[64,2,512]{2,1,0:T(2,128)} %broadcast_in_dim.183), calls=%async_computation.1 | async-start | bytes 524288 | tf_op jit(solution)/shard_map/all_to_all | solution.py:25
  221.7 6.9 %fusion.67 = f32[2,512,128]{1,2,0:T(8,128)S(1)} fusion(bf16[2,128,128]{2,1,0:T(8,128)(2,1)S(1)} %copy-done, bf16[512,256]{1,0:T(8,128)(2,1)} %copy-done.9, s32[256]{0:T(256)S(1)} %copy-done.21, s32[512]{0:T(512)S(1)} %copy-done.16, f32[528,256]{1,0:T(8,128)} %maximum_convert_fusion.1, pred[256]{0:T(512)(128)(4,1)S(1)} %copy-done.36, ...), kind=kOutput, calls=%fused_computation.96 | convolution fusion | flops 38404096 | bytes 9248000 | tf_op jit(solution)/shard_map/tgc,gcd->tgd/dot_general | solution.py:165
  228.8 4.1 %fusion.36 = f32[512,2048]{1,0:T(8,128)} fusion(bf16[512,256]{0,1:T(8,128)(2,1)S(1)} %fusion.59, bf16[2048,2048]{1,0:T(8,128)(2,1)} %all-gather.2.cloned.1.call-done), kind=kOutput, calls=%fused_computation.41 | convolution fusion | flops 536870912 | bytes 5505024 | tf_op jit(solution)/shard_map/dot_general | solution.py:103
  236.8 9.2 %convolution_add_fusion = f32[512,2048]{1,0:T(8,128)} fusion(f32[512,2048]{1,0:T(8,128)} %fusion.36, bf16[2048,2048]{1,0:T(8,128)(2,1)} %all-gather.2.cloned.1.call-done, bf16[512,2048]{1,0:T(8,128)(2,1)S(1)} %copy-done.1, f32[512,512]{1,0:T(8,128)S(1)} %pad.144, f32[512,512]{1,0:T(8,128)} %pad.145, f32[512,512]{1,0:T(8,128)} %pad.126, ...), kind=kOutput, calls=%fused_computation.4 | convolution fusion | flops 2152726528 | bytes 18876416 | tf_op jit(solution)/shard_map/dot_general | solution.py:103
  245.9 15.0 %all_to_all.15 = f32[2,256,2048]{2,1,0:T(8,128)} all-to-all(f32[2,256,2048]{2,1,0:T(8,128)} %bitcast.48), channel_id=1, replica_groups=mesh['sp'=64,'fs'=4,'tp'=2] {'tp'}, dimensions={0} | all-to-all | bytes 8388608 | tf_op jit(solution)/shard_map/all_to_all | solution.py:94
  261.0 3.8 %reduce_sum.19 = bf16[256,2048]{1,0:T(8,128)(2,1)} reduce(f32[2,256,2048]{2,1,0:T(8,128)} %all_to_all.15, f32[]{:T(128)} %constant.95.clone.1), dimensions={0}, to_apply=%region_1.2 | reduce | flops 524288 | bytes 5242884 | tf_op jit(solution)/shard_map/reduce_sum | solution.py:95
  (254 shorter events, 24.2 us)
Async XLA Ops:
  6.5 215.0 %copy-start = (bf16[2,128,128]{2,1,0:T(8,128)(2,1)S(1)}, bf16[2,128,128]{2,1,0:T(8,128)(2,1)}, u32[]{:S(2)}) copy-start(bf16[2,128,128]{2,1,0:T(8,128)(2,1)} %param.20) | copy-start | bytes 196612
  6.5 108.9 %all-gather.2.cloned.1.call-start = ((), (), s32[]{:S(2)}) async-start(), calls=%async_computation.3 | async-start | bytes 8519680 | tf_op jit(solution)/shard_map/all_gather | solution.py:19
  10.3 0.7 copy-start.10
  13.8 13.1 %all-to-all-start = ((bf16[2,256,2048]{2,1,0:T(8,128)(2,1)}), bf16[2,256,2048]{2,1,0:T(8,128)(2,1)S(1)}, u32[]{:S(2)}, u32[]{:S(2)}) async-start(bf16[2,256,2048]{2,1,0:T(8,128)(2,1)} %broadcast_in_dim.164), calls=%async_computation | async-start | bytes 4194304 | tf_op jit(solution)/shard_map/all_to_all | solution.py:25
  24.4 8.6 %copy-start.17 = (f32[512]{0:T(512)S(1)}, f32[512]{0:T(512)}, u32[]{:S(2)}) copy-start(f32[512]{0:T(512)} %param.25) | copy-start | bytes 6148
  24.4 8.7 %copy-start.15 = (f32[4,512]{1,0:T(4,128)S(1)}, f32[4,512]{1,0:T(4,128)}, u32[]{:S(2)}) copy-start(f32[4,512]{1,0:T(4,128)} %param.22) | copy-start | bytes 24580
  24.4 8.7 %copy-start.14 = (f32[2048]{0:T(1024)S(1)}, f32[2048]{0:T(1024)}, u32[]{:S(2)}) copy-start(f32[2048]{0:T(1024)} %param.16) | copy-start | bytes 24580
  34.9 83.8 %copy-start.1 = (bf16[512,2048]{1,0:T(8,128)(2,1)S(1)}, bf16[512,2048]{1,0:T(8,128)(2,1)}, u32[]{:S(2)}) copy-start(bf16[512,2048]{1,0:T(8,128)(2,1)} %fusion.1) | copy-start | bytes 6291460
  118.0 0.7 copy-start.9
  118.7 6.7 %copy-start.13 = (f32[8,512]{1,0:T(8,128)S(1)}, f32[8,512]{1,0:T(8,128)}, u32[]{:S(2)}) copy-start(f32[8,512]{1,0:T(8,128)} %param.26) | copy-start | bytes 49156
  121.6 3.9 %copy-start.8 = (bf16[512,512]{1,0:T(8,128)(2,1)}, bf16[512,512]{1,0:T(8,128)(2,1)S(1)}, u32[]{:S(2)}) copy-start(bf16[512,512]{1,0:T(8,128)(2,1)S(1)} %fusion.7) | copy-start | bytes 1572868
  121.6 5.3 %collective-permute-start = (bf16[16,768]{1,0:T(8,128)(2,1)S(1)}, bf16[16,768]{1,0:T(8,128)(2,1)S(1)}, u32[]{:S(2)}, u32[]{:S(2)}) collective-permute-start(bf16[16,768]{1,0:T(8,128)(2,1)S(1)} %pad_maximum_fusion.10), channel_id=1, source_target_pairs={{0,8},{8,16},{16,24},{24,32},{32,40},{40,48},{48,56},{56,64},{64,7... | collective-permute-start | bytes 73736 | tf_op jit(solution)/shard_map/ppermute | solution.py:44
  128.1 3.3 %copy-start.11 = (bf16[8,64,64]{2,1,0:T(8,128)(2,1)S(1)}, bf16[8,64,64]{2,1,0:T(8,128)(2,1)}, u32[]{:S(2)}) copy-start(bf16[8,64,64]{2,1,0:T(8,128)(2,1)} %param.24) | copy-start | bytes 196612
  128.1 3.3 %copy-start.12 = (bf16[8,64,64]{2,1,0:T(8,128)(2,1)S(1)}, bf16[8,64,64]{2,1,0:T(8,128)(2,1)}, u32[]{:S(2)}) copy-start(bf16[8,64,64]{2,1,0:T(8,128)(2,1)} %param.23) | copy-start | bytes 196612
  144.1 1.0 copy-start.3
  144.1 12.0 %copy-start.2 = (f32[512,512]{1,0:T(8,128)S(1)}, f32[512,512]{1,0:T(8,128)}, u32[]{:S(2)}) copy-start(f32[512,512]{1,0:T(8,128)} %get-tuple-element.6) | copy-start | bytes 3145732
  184.7 4.0 %copy-start.4 = (f32[256,512]{1,0:T(8,128)S(1)}, f32[256,512]{1,0:T(8,128)}, u32[]{:S(2)}) copy-start(f32[256,512]{1,0:T(8,128)} %pad.125) | copy-start | bytes 1572868
  184.7 4.0 %copy-start.5 = (f32[256,512]{1,0:T(8,128)S(1)}, f32[256,512]{1,0:T(8,128)}, u32[]{:S(2)}) copy-start(f32[256,512]{1,0:T(8,128)} %pad.143) | copy-start | bytes 1572868
  184.7 4.0 %copy-start.6 = (f32[255,512]{1,0:T(8,128)S(1)}, f32[255,512]{1,0:T(8,128)}, u32[]{:S(2)}) copy-start(f32[255,512]{1,0:T(8,128)} %slice.534) | copy-start | bytes 1566724
  184.7 4.0 %copy-start.7 = (f32[255,512]{1,0:T(8,128)S(1)}, f32[255,512]{1,0:T(8,128)}, u32[]{:S(2)}) copy-start(f32[255,512]{1,0:T(8,128)} %slice.469) | copy-start | bytes 1566724
  199.4 22.1 %copy-start.16 = (s32[512]{0:T(512)S(1)}, s32[512]{0:T(512)}, u32[]{:S(2)}) copy-start(s32[512]{0:T(512)} %add_add_fusion) | copy-start | bytes 6148
  199.4 22.2 %copy-start.21 = (s32[256]{0:T(256)S(1)}, s32[256]{0:T(256)}, u32[]{:S(2)}) copy-start(s32[256]{0:T(256)} %fusion.87) | copy-start | bytes 3076
  199.4 22.2 %copy-start.22 = (pred[256]{0:T(512)(128)(4,1)S(1)}, pred[256]{0:T(512)(128)(4,1)}, u32[]{:S(2)}) copy-start(pred[256]{0:T(512)(128)(4,1)} %get-tuple-element.77) | copy-start | bytes 772
  199.4 22.2 %copy-start.23 = (pred[256]{0:T(512)(128)(4,1)S(1)}, pred[256]{0:T(512)(128)(4,1)}, u32[]{:S(2)}) copy-start(pred[256]{0:T(512)(128)(4,1)} %get-tuple-element.78) | copy-start | bytes 772
  199.4 22.2 %copy-start.24 = (pred[256]{0:T(512)(128)(4,1)S(1)}, pred[256]{0:T(512)(128)(4,1)}, u32[]{:S(2)}) copy-start(pred[256]{0:T(512)(128)(4,1)} %get-tuple-element.73) | copy-start | bytes 772
  199.4 22.2 %copy-start.25 = (pred[256]{0:T(512)(128)(4,1)S(1)}, pred[256]{0:T(512)(128)(4,1)}, u32[]{:S(2)}) copy-start(pred[256]{0:T(512)(128)(4,1)} %get-tuple-element.74) | copy-start | bytes 772
  199.4 22.2 %copy-start.26 = (pred[256]{0:T(512)(128)(4,1)S(1)}, pred[256]{0:T(512)(128)(4,1)}, u32[]{:S(2)}) copy-start(pred[256]{0:T(512)(128)(4,1)} %get-tuple-element.79) | copy-start | bytes 772
  199.4 22.2 %copy-start.27 = (pred[256]{0:T(512)(128)(4,1)S(1)}, pred[256]{0:T(512)(128)(4,1)}, u32[]{:S(2)}) copy-start(pred[256]{0:T(512)(128)(4,1)} %get-tuple-element.80) | copy-start | bytes 772
  199.4 22.2 %copy-start.28 = (pred[256]{0:T(512)(128)(4,1)S(1)}, pred[256]{0:T(512)(128)(4,1)}, u32[]{:S(2)}) copy-start(pred[256]{0:T(512)(128)(4,1)} %get-tuple-element.71) | copy-start | bytes 772
  199.5 22.2 %copy-start.29 = (pred[256]{0:T(512)(128)(4,1)S(1)}, pred[256]{0:T(512)(128)(4,1)}, u32[]{:S(2)}) copy-start(pred[256]{0:T(512)(128)(4,1)} %get-tuple-element.72) | copy-start | bytes 772
  199.5 22.2 %copy-start.30 = (pred[256]{0:T(512)(128)(4,1)S(1)}, pred[256]{0:T(512)(128)(4,1)}, u32[]{:S(2)}) copy-start(pred[256]{0:T(512)(128)(4,1)} %get-tuple-element.81) | copy-start | bytes 772
  199.5 22.2 %copy-start.31 = (pred[256]{0:T(512)(128)(4,1)S(1)}, pred[256]{0:T(512)(128)(4,1)}, u32[]{:S(2)}) copy-start(pred[256]{0:T(512)(128)(4,1)} %get-tuple-element.82) | copy-start | bytes 772
  199.5 22.2 %copy-start.32 = (pred[256]{0:T(512)(128)(4,1)S(1)}, pred[256]{0:T(512)(128)(4,1)}, u32[]{:S(2)}) copy-start(pred[256]{0:T(512)(128)(4,1)} %get-tuple-element.69) | copy-start | bytes 772
  199.5 22.2 %copy-start.33 = (pred[256]{0:T(512)(128)(4,1)S(1)}, pred[256]{0:T(512)(128)(4,1)}, u32[]{:S(2)}) copy-start(pred[256]{0:T(512)(128)(4,1)} %get-tuple-element.70) | copy-start | bytes 772
  199.5 22.2 %copy-start.34 = (pred[256]{0:T(512)(128)(4,1)S(1)}, pred[256]{0:T(512)(128)(4,1)}, u32[]{:S(2)}) copy-start(pred[256]{0:T(512)(128)(4,1)} %get-tuple-element.75) | copy-start | bytes 772
  199.5 22.2 %copy-start.35 = (pred[256]{0:T(512)(128)(4,1)S(1)}, pred[256]{0:T(512)(128)(4,1)}, u32[]{:S(2)}) copy-start(pred[256]{0:T(512)(128)(4,1)} %get-tuple-element.76) | copy-start | bytes 772
  199.5 22.2 %copy-start.36 = (pred[256]{0:T(512)(128)(4,1)S(1)}, pred[256]{0:T(512)(128)(4,1)}, u32[]{:S(2)}) copy-start(pred[256]{0:T(512)(128)(4,1)} %get-tuple-element.67) | copy-start | bytes 772
  211.0 22.8 %all-to-all-start.1 = ((f32[64,2,512]{2,1,0:T(2,128)}), f32[64,2,512]{2,1,0:T(2,128)S(1)}, u32[]{:S(2)}, u32[]{:S(2)}) async-start(f32[64,2,512]{2,1,0:T(2,128)} %broadcast_in_dim.183), calls=%async_computation.1 | async-start | bytes 524288 | tf_op jit(solution)/shard_map/all_to_all | solution.py:25
  221.7 7.0 %copy-start.19 = (f32[256]{0:T(256)S(1)}, f32[256]{0:T(256)}, u32[]{:S(2)}) copy-start(f32[256]{0:T(256)} %param.21) | copy-start | bytes 3076
  228.8 5.2 %copy-start.20 = (pred[64]{0:T(512)(128)(4,1)S(1)}, pred[64]{0:T(512)(128)(4,1)}, u32[]{:S(2)}) copy-start(pred[64]{0:T(512)(128)(4,1)} %iota_compare_fusion) | copy-start | bytes 196
  232.9 3.9 %copy-start.18 = (f32[512]{0:T(512)S(1)}, f32[512]{0:T(512)}, u32[]{:S(2)}) copy-start(f32[512]{0:T(512)} %param.27) | copy-start | bytes 6148
Sparse Core Ops, SparseCore 0:
  11.1 104.3 all-gather.1
where the time goes:
time: 274 us; the launch traced here: 272 us
  waiting for transfers between devices  83.9 us (31%)
  local copies, waits for them, and re-layouts  65.8 us (24%)
  other arithmetic  40.6 us (15%)
  matrix products  27.2 us (10%)
  starting transfers between devices  24.4 us (9%)
  blocking collectives  15 us (5%)
  between operations  14.6 us (5%)
    all_gather x1, waiting for transfers between devices, sent_together(): result = lax.all_gather(both, axis, axis=dim, tiled=True)  80.5 us
    slice x60, local copies, waits for them, and re-layouts, shards(): lax.associative_scan(chain_pairs, (decays, drives), axis=0)  23.8 us
    pad x32, local copies, waits for them, and re-layouts, shards(): lax.associative_scan(chain_pairs, (decays, drives), axis=0)  21.8 us
    all_to_all x2, starting transfers between devices, from_everyone(): lax.all_to_all(jnp.broadcast_to(array[None], (count, *array.shape)), axis...  21.1 us
    all_to_all x1, blocking collectives, sent_and_summed(): lax.all_to_all(parts, axis, split_axis=0, concat_axis=0, tiled=True)  15 us
    dot_general x2, matrix products, right_product(): lax.dot_general(left_rows, weight_rows, (((1,), (1,)), ((), ())), preferr...  13.3 us
    dot_general x1, matrix products, shards(): jnp.einsum('tgc,gcd->tgd', grouped, pool_mix, preferred_element_type=jnp....  6.94 us
    add x17, other arithmetic, shards(): lax.associative_scan(chain_pairs, (decays, drives), axis=0)  6.35 us
  transfers between devices with their start and end apart: 4, of which 3 were waited for; matrix products, arithmetic and copies ran while one was open for 9% of the time, Pallas kernels for 0%

commit v1 on v0

v1 whole, which is shorter than its diff:
```python
import functools
import math

import jax
import jax.numpy as jnp
from jax import lax
from jax.experimental import pallas as pl
from jax.experimental.pallas import tpu as pltpu
from jax.sharding import PartitionSpec as P

HEAD = 64
LANES = 128
REACH = 16
SEGMENTS = 8
EPSILON = 1e-06
SHARPNESS = 8.0
MESH = pl.DeviceIdType.MESH
F32 = jnp.float32
BF16 = jnp.bfloat16

VALUE = 0
GATES = (512, 896)
POOLS = (768, 1152)
OUT = 1280
PACKED = 2048
WINDOWS = (
    ((0, 256), (512, 384), (1280, 256), (1536, 128)),
    ((256, 256), (896, 384), (1664, 256), (1920, 128)),
)
STARTS = (0, 1, 4, 5)
JOBS = len(STARTS)


def wrapped(index, count):
    return lax.rem(index + count, count)


def log1p_of_exp(v):
    e = jnp.exp(-jnp.abs(v))
    s = e / (2.0 + e)
    q = s * s
    total = jnp.full_like(q, 1.0 / 15.0)
    for odd in (13, 11, 9, 7, 5, 3, 1):
        total = total * q + 1.0 / odd
    return jnp.maximum(v, 0.0) + 2.0 * s * total


def one_minus_exp(y):
    series = jnp.full_like(y, 1.0)
    for k in (9, 8, 7, 6, 5, 4, 3, 2):
        series = 1.0 + series * y * (1.0 / k)
    return jnp.where(y > -0.6, -y * series, 1.0 - jnp.exp(y))


def kernel(ny, nz, *refs):
    (tok_in, gain_in, pool_in, gate_in, value_in, pmix_in, avg_in, taps_in, rmix_in, imix_in,
     lrate_in, shift_in, init_in, opool_in, ornn_in, out,
     w, tok, nrm, proj, aa, bb, acts, shift_t, gain, pmix, avg, taps, rmix, imix, lrate, shift,
     init, bd, soft, ends_a, ends_b, enter, ybuf, zbuf, psend, precv, obuf,
     local_sem, ring_send, ring_recv, pair_send, pair_recv, next_send, next_recv,
     y_send, y_recv, z_send, z_recv, part_send, part_recv, out_sem) = refs
    half, depth = tok_in.shape
    rows = 2 * half
    seg = rows // SEGMENTS
    rnn = lrate.shape[1]
    sp, tp = lax.axis_index("sp"), lax.axis_index("tp")
    z, y = sp // ny, lax.rem(sp, ny)
    count = ny * nz

    def at_y(k):
        return z * ny + wrapped(y + k, ny)

    def at_z(k):
        return wrapped(z + k, nz) * ny + y

    def local(k, src, dst):
        return pltpu.make_async_copy(src, dst, local_sem.at[k])

    mine = w.at[z, y]
    packing = [
        local(0, value_in, mine.at[:, 0:512]),
        local(1, gate_in.at[:, 0:256], mine.at[:, 512:768]),
        local(2, pool_in.at[:, 0:128], mine.at[:, 768:896]),
        local(3, gate_in.at[:, 256:512], mine.at[:, 896:1152]),
        local(4, pool_in.at[:, 128:256], mine.at[:, 1152:1280]),
        local(5, ornn_in, mine.at[:, 1280:1792]),
        local(6, opool_in, mine.at[:, 1792:2048]),
    ]
    my_rows = pl.ds(pl.multiple_of(REACH + tp * half, REACH), half)
    own_tokens = local(7, tok_in, tok.at[my_rows])
    small = [
        local(8 + k, src, dst)
        for k, (src, dst) in enumerate(
            [(gain_in, gain), (pmix_in, pmix), (avg_in, avg), (taps_in, taps), (rmix_in, rmix),
             (imix_in, imix), (lrate_in, lrate), (shift_in, shift), (init_in, init)]
        )
    ]
    for copy in packing + [own_tokens] + small:
        copy.start()

    barrier = pltpu.get_barrier_semaphore()
    peers = [at_y(k) for k in range(1, ny)] + [at_z(k) for k in range(1, nz)]
    peers += [wrapped(sp + 1, count), wrapped(sp - 1, count)]
    for peer in peers:
        pl.semaphore_signal(barrier, inc=1, device_id={"sp": peer}, device_id_type=MESH)
    pl.semaphore_signal(barrier, inc=1, device_id={"tp": 1 - tp}, device_id_type=MESH)
    pl.semaphore_wait(barrier, len(peers) + 1)

    pair = pltpu.make_async_remote_copy(
        src_ref=tok_in, dst_ref=tok.at[my_rows], send_sem=pair_send, recv_sem=pair_recv,
        device_id={"tp": 1 - tp}, device_id_type=MESH,
    )
    pair.start()
    halo = pltpu.make_async_remote_copy(
        src_ref=tok.at[pl.ds(rows, REACH)], dst_ref=tok.at[pl.ds(0, REACH)],
        send_sem=next_send, recv_sem=next_recv,
        device_id={"sp": wrapped(sp + 1, count)}, device_id_type=MESH,
    )

    sizes = ((ny, nz), (nz, ny))
    homes = ((y, z), (z, y))

    def hops(color, job, phase, way):
        n = sizes[color][phase]
        return n // 2 if (way + job + color) % 2 == 0 else (n - 1) // 2

    def block(color, job, phase, origin):
        first, width = WINDOWS[color][job]
        cols = pl.ds(first, width)
        if color == 0:
            return w.at[z, origin, :, cols] if phase == 0 else w.at[origin, :, :, cols]
        return w.at[origin, y, :, cols] if phase == 0 else w.at[:, origin, :, cols]

    def ring(color, job, phase, way, step, arriving):
        n = sizes[color][phase]
        home = homes[color][phase]
        back = step + 1 if arriving else step
        origin = wrapped(home - back if way == 0 else home + back, n)
        on_y = (color == 0) == (phase == 0)
        ahead = 1 if way == 0 else -1
        ref = block(color, job, phase, origin)
        return pltpu.make_async_remote_copy(
            src_ref=ref, dst_ref=ref,
            send_sem=ring_send.at[color, job, phase, way, step],
            recv_sem=ring_recv.at[color, job, phase, way, step],
            device_id={"sp": at_y(ahead) if on_y else at_z(ahead)}, device_id_type=MESH,
        )

    def steps_of(color, job):
        result = []
        for phase in (0, 1):
            for step in range(max(hops(color, job, phase, 0), hops(color, job, phase, 1))):
                result.append([
                    (color, job, phase, way, step) for way in (0, 1)
                    if step < hops(color, job, phase, way)
                ])
        return result

    plans = {(c, j): steps_of(c, j) for c in (0, 1) for j in range(JOBS)}
    started = []

    def advance(color, job, at):
        plan = plans[color, job]
        if 0 < at <= len(plan):
            for key in plan[at - 1]:
                ring(*key, True).wait_recv()
        if 0 <= at < len(plan):
            for key in plan[at]:
                ring(*key, False).start()
                started.append(key)

    def round_of(r):
        if r == 0:
            packing[0].wait()
        if r == STARTS[1]:
            for copy in packing[1:]:
                copy.wait()
        for job in range(JOBS):
            for color in (0, 1):
                advance(color, job, r - STARTS[job])

    def prepare():
        for copy in small:
            copy.wait()
        lane = lax.broadcasted_iota(jnp.int32, (HEAD, LANES), 1)
        for k in range(rnn // LANES):
            for side, mix in enumerate((rmix, imix)):
                both = jnp.concatenate(
                    [mix[2 * k].astype(F32), mix[2 * k + 1].astype(F32)], axis=1
                )
                cols = slice(side * LANES, (side + 1) * LANES)
                bd[k, 0:HEAD, cols] = jnp.where(lane < HEAD, both, 0.0).astype(BF16)
                bd[k, HEAD:LANES, cols] = jnp.where(lane < HEAD, 0.0, both).astype(BF16)
        soft[...] = log1p_of_exp(-lrate[...]) * (-SHARPNESS)
        shift_t[...] = shift[...].T

    def normalize(first, last):
        def body(i, carry):
            at = pl.ds(pl.multiple_of(i * REACH, REACH), REACH)
            x = tok[at, :].astype(F32)
            mean = jnp.sum(x * x, axis=1, keepdims=True) * (1.0 / depth)
            keep = jnp.where(jnp.logical_and(i == 0, sp == 0), 0.0, 1.0)
            nrm[at, :] = (x * lax.rsqrt(mean + EPSILON) * gain[...] * keep).astype(BF16)
            return carry
        lax.fori_loop(first, last, body, 0)

    def project(first, last):
        def body(n, carry):
            cols = pl.ds(pl.multiple_of(n * 256, 256), 256)
            weight = w[:, :, :, cols].reshape(depth, 256)
            result = jnp.dot(nrm[...], weight, preferred_element_type=F32)
            proj[:, cols] = result.astype(BF16).astype(F32)
            return carry
        lax.fori_loop(first, last, body, 0)

    def gates():
        low = lax.broadcasted_iota(jnp.int32, (seg, LANES), 1) < HEAD

        def body(i, carry):
            first = pl.multiple_of(i * seg, seg)
            at = pl.ds(first, seg)
            for k in range(rnn // LANES):
                cols = slice(k * LANES, (k + 1) * LANES)
                v = proj[pl.ds(first, seg + REACH), cols]
                conv = taps[0:1, cols] * v[13:13 + seg]
                for tap in (1, 2, 3):
                    conv = conv + taps[tap:tap + 1, cols] * v[13 + tap:13 + tap + seg]
                conv = conv.astype(BF16)
                terms = jnp.dot(conv, bd[k], preferred_element_type=F32)
                rate = jax.nn.sigmoid(terms[:, :LANES])
                entry = jax.nn.sigmoid(terms[:, LANES:])
                shifts = jnp.where(
                    low, shift_t[at, 2 * k:2 * k + 1], shift_t[at, 2 * k + 1:2 * k + 2]
                )
                log_decay = rate * soft[0:1, cols] + shifts
                aa[k, at, :] = jnp.exp(log_decay)
                bb[k, at, :] = (
                    jnp.sqrt(one_minus_exp(2.0 * log_decay)) * entry * conv.astype(F32)
                )
            return carry
        lax.fori_loop(0, SEGMENTS, body, 0)

    def scan():
        tiles = range(rnn // LANES)

        def body(j, carry):
            at = pl.ds(j, SEGMENTS, stride=seg)
            result = []
            for k in tiles:
                decay, state = carry[k]
                a, b = aa[k, at, :], bb[k, at, :]
                decay = decay * a
                state = a * state + b
                aa[k, at, :] = decay
                bb[k, at, :] = state
                result.append((decay, state))
            return tuple(result)
        start = (jnp.ones((SEGMENTS, LANES), F32), jnp.zeros((SEGMENTS, LANES), F32))
        for k, (decay, state) in enumerate(lax.fori_loop(0, seg, body, (start,) * len(tiles))):
            ends_a[:, k * LANES:(k + 1) * LANES] = decay
            ends_b[:, k * LANES:(k + 1) * LANES] = state
        total_a, total_b = jnp.ones((1, rnn), F32), jnp.zeros((1, rnn), F32)
        for s in range(SEGMENTS):
            enter[s, :, 0:rnn] = total_a
            enter[s, :, rnn:] = total_b
            a, b = ends_a[s:s + 1, :], ends_b[s:s + 1, :]
            total_a, total_b = total_a * a, a * total_b + b
        ybuf[y, :, 0:rnn] = total_a
        ybuf[y, :, rnn:] = total_b

    def to_others(buf, home, n, sends, recvs, target, k, arriving):
        slot = buf.at[wrapped(home - k, n) if arriving else home]
        return pltpu.make_async_remote_copy(
            src_ref=slot, dst_ref=slot, send_sem=sends.at[k], recv_sem=recvs.at[k],
            device_id={"sp": target(k)}, device_id_type=MESH,
        )

    def y_copy(k, arriving):
        return to_others(ybuf, y, ny, y_send, y_recv, at_y, k, arriving)

    def z_copy(k, arriving):
        return to_others(zbuf, z, nz, z_send, z_recv, at_z, k, arriving)

    def chained(buf, n, home):
        whole = before = (jnp.ones((1, rnn), F32), jnp.zeros((1, rnn), F32))
        for s in range(n):
            a, b = buf[s, :, 0:rnn], buf[s, :, rnn:]
            before = tuple(jnp.where(s == home, new, old) for new, old in zip(whole, before))
            whole = (whole[0] * a, a * whole[1] + b)
        return whole, before

    def pool():
        def body(i, carry):
            first = pl.multiple_of(i * seg, seg)
            at = pl.ds(first, seg)
            place = sp * rows + first + lax.broadcasted_iota(jnp.int32, (seg, LANES), 0)
            for g in (0, 1):
                x = proj[pl.ds(first, seg + REACH), POOLS[g]:POOLS[g] + LANES]
                near = x + pltpu.roll(x, 1, 0)
                if g == 1:
                    near = near + pltpu.roll(near, 2, 0)
                far = near
                for width in ((2, 4) if g == 0 else (4, 8)):
                    far = far + pltpu.roll(far, width, 0)
                window = jnp.where(tp == 0, 2 << g, 8 << g)
                summed = jnp.where(tp == 0, near, far)[REACH:]
                counts = jnp.minimum(place + 1, window).astype(F32)
                pooled = (summed / counts - x[REACH:]).astype(BF16)
                mixed = jnp.dot(pooled, pmix[g], preferred_element_type=F32)
                cols = slice(g * LANES, (g + 1) * LANES)
                acts[at, rnn + g * LANES:rnn + (g + 1) * LANES] = (
                    mixed * avg[0:1, cols]
                ).astype(BF16)
            return carry
        lax.fori_loop(0, SEGMENTS, body, 0)

    def gelu():
        scale = math.sqrt(2.0 / math.pi)

        def body(i, carry):
            at = pl.ds(pl.multiple_of(REACH + i * seg, REACH), seg)
            for g in (0, 1):
                cols = slice(GATES[g], GATES[g] + 256)
                x = proj[at, cols]
                proj[at, cols] = x * (
                    0.5 * (1.0 + jnp.tanh(scale * (x + 0.044715 * (x * x * x))))
                )
            return carry
        lax.fori_loop(0, SEGMENTS, body, 0)

    def finish(carried):
        def body(i, carry):
            first = pl.multiple_of(i * seg, seg)
            at = pl.ds(first, seg)
            begin = enter[i, :, 0:rnn] * carried + enter[i, :, rnn:]
            for k in range(rnn // LANES):
                cols = slice(k * LANES, (k + 1) * LANES)
                state = bb[k, at, :] + aa[k, at, :] * begin[:, cols]
                column = GATES[k // 2] + k % 2 * LANES
                gate = proj[pl.ds(pl.multiple_of(REACH + first, REACH), seg),
                            column:column + LANES]
                acts[at, cols] = (gate * state).astype(BF16)
            return carry
        lax.fori_loop(0, SEGMENTS, body, 0)

    features = ny * w.shape[2]

    def part_copy(n):
        return pltpu.make_async_remote_copy(
            src_ref=psend.at[n], dst_ref=precv.at[n], send_sem=part_send.at[n],
            recv_sem=part_recv.at[n], device_id={"tp": 1 - tp}, device_id_type=MESH,
        )

    def product(side, n):
        at = pl.ds(pl.multiple_of(side * half, REACH), half)
        weight = w[n, :, :, OUT:PACKED].reshape(features, PACKED - OUT)
        return lax.dot_general(
            acts[at, :], weight, (((1,), (1,)), ((), ())), preferred_element_type=F32
        )

    def out_copy(n):
        return pltpu.make_async_copy(
            obuf.at[n], out.at[:, pl.ds(pl.multiple_of(n * features, LANES), features)],
            out_sem.at[n],
        )

    round_of(0)
    own_tokens.wait()
    pair.wait_recv()
    halo.start()
    round_of(1)
    prepare()
    round_of(2)
    halo.wait_recv()
    normalize(0, 17)
    round_of(3)
    normalize(17, (rows + REACH) // REACH)
    plan_len = max(len(p) for p in plans.values())
    for r in range(4, plan_len + 1):
        round_of(r)
    project(0, 2)
    round_of(plan_len + 1)
    gates()
    round_of(plan_len + 2)
    scan()
    for k in range(1, ny):
        y_copy(k, False).start()
    round_of(plan_len + 3)
    project(2, 5)
    for k in range(1, ny):
        y_copy(k, True).wait_recv()
    whole, in_row = chained(ybuf, ny, y)
    zbuf[z, :, 0:rnn] = whole[0]
    zbuf[z, :, rnn:] = whole[1]
    for k in range(1, nz):
        z_copy(k, False).start()
    round_of(plan_len + 4)
    pool()
    gelu()
    round_of(plan_len + 5)
    for k in range(1, nz):
        z_copy(k, True).wait_recv()
    _, rows_before = chained(zbuf, nz, z)
    carried = in_row[0] * (rows_before[0] * init[...] + rows_before[1]) + in_row[1]
    finish(carried)

    def to_partner(n, carry):
        psend[n] = product(1 - tp, n).astype(BF16)
        part_copy(n).start()
        return carry

    lax.fori_loop(0, nz, to_partner, 0)

    def for_me(n, carry):
        own = product(tp, n)
        part_copy(n).wait_recv()
        obuf[n] = (own + precv[n].astype(F32)).astype(BF16)
        out_copy(n).start()
        return carry

    lax.fori_loop(0, nz, for_me, 0)

    for key in started:
        ring(*key, False).wait_send()
    pair.wait_send()
    halo.wait_send()
    for k in range(1, ny):
        y_copy(k, False).wait_send()
    for k in range(1, nz):
        z_copy(k, False).wait_send()

    def ended(n, carry):
        part_copy(n).wait_send()
        out_copy(n).wait()
        return carry

    lax.fori_loop(0, nz, ended, 0)


def shards(ny, nz, tokens, norm_gain, pool_in, gate_in, value_in, pool_mix, averaging_factor,
           conv_taps, rate_mix, input_mix, log_rate, decay_shift, initial_state, out_pool,
           out_rnn):
    half, depth = tokens.shape
    rows = 2 * half
    rnn = log_rate.shape[0]
    lines = pool_in.shape[0]
    features = ny * lines
    steps = max(ny, nz) // 2
    dma = pltpu.SemaphoreType.DMA
    vmem = pltpu.VMEM
    scratch = [
        vmem((nz, ny, lines, PACKED), BF16),
        vmem((rows + REACH, depth), BF16),
        vmem((rows + REACH, depth), BF16),
        vmem((rows + REACH, OUT), F32),
        vmem((rnn // LANES, rows, LANES), F32),
        vmem((rnn // LANES, rows, LANES), F32),
        vmem((rows, PACKED - OUT), BF16),
        vmem((rows, rnn // HEAD), F32),
        vmem((1, depth), F32),
        vmem(pool_mix.shape, BF16),
        vmem((1, 2 * LANES), F32),
        vmem(conv_taps.shape, F32),
        vmem(rate_mix.shape, BF16),
        vmem(input_mix.shape, BF16),
        vmem((1, rnn), F32),
        vmem(decay_shift.shape, F32),
        vmem((1, rnn), F32),
        vmem((rnn // LANES, LANES, 2 * LANES), BF16),
        vmem((1, rnn), F32),
        vmem((SEGMENTS, rnn), F32),
        vmem((SEGMENTS, rnn), F32),
        vmem((SEGMENTS, 1, 2 * rnn), F32),
        vmem((ny, 1, 2 * rnn), F32),
        vmem((nz, 1, 2 * rnn), F32),
        vmem((nz, half, features), BF16),
        vmem((nz, half, features), BF16),
        vmem((nz, half, features), BF16),
        dma((17,)),
        dma((2, JOBS, 2, 2, steps)),
        dma((2, JOBS, 2, 2, steps)),
        dma, dma, dma, dma,
        dma((ny,)), dma((ny,)), dma((nz,)), dma((nz,)),
        dma((nz,)), dma((nz,)), dma((nz,)),
    ]
    anywhere = pl.BlockSpec(memory_space=pl.ANY)
    return pl.pallas_call(
        functools.partial(kernel, ny, nz),
        out_shape=jax.ShapeDtypeStruct((half, depth), BF16),
        in_specs=[anywhere] * 15,
        out_specs=anywhere,
        scratch_shapes=scratch,
        compiler_params=pltpu.CompilerParams(
            collective_id=0, has_side_effects=True, vmem_limit_bytes=56 * 1024 * 1024
        ),
        name="layer",
    )(tokens, norm_gain[None], pool_in, gate_in, value_in, pool_mix, averaging_factor[None],
      conv_taps, rate_mix, input_mix, log_rate[None], decay_shift, initial_state[None], out_pool,
      out_rnn)


def grid_of(count):
    ny = 1
    while ny * ny < count:
        ny *= 2
    return ny, count // ny


def solution(mesh):
    ny, nz = grid_of(mesh.shape["sp"])
    placed = (
        P(("fs", "sp", "tp"), None),
        P(),
        P("sp", "tp"),
        P("sp", "tp"),
        P("sp", "tp"),
        P("tp", None, None),
        P("tp"),
        P(None, "tp"),
        P("tp", None, None),
        P("tp", None, None),
        P("tp"),
        P(("fs", "tp"), "sp"),
        P(("fs", "tp")),
        P("sp", "tp"),
        P("sp", "tp"),
    )
    return jax.shard_map(
        functools.partial(shards, ny, nz), mesh=mesh, in_specs=placed,
        out_specs=P(("fs", "sp", "tp"), None), check_vma=False,
    )
```

time: 274 us -> 95.7 us (0.35)
  Pallas kernels: 0 us -> 93.2 us
  waiting for transfers between devices: 83.9 us -> 0 us
  local copies, waits for them, and re-layouts: 65.8 us -> 2.3 us
  other arithmetic: 40.6 us -> 0 us
  matrix products: 27.2 us -> 0 us
  starting transfers between devices: 24.4 us -> 0 us
  blocking collectives: 15 us -> 0 us
  between operations: 14.6 us -> 0.01 us
    pallas_call x0 -> x1, Pallas kernels: none -> 93.2 us  [shards(): pl.pallas_call(functools.partial(kernel, ny, nz), out_shape=jax.ShapeDtyp...]
    all_gather x1 -> x0, waiting for transfers between devices: 80.5 us -> none  [sent_together(): result = lax.all_gather(both, axis, axis=dim, tiled=True)]
    dot_general x6 -> x0, matrix products: 27.2 us -> none  [the longest x2 13.3 us: right_product(): lax.dot_general(left_rows, weight_rows, (((1,), (1,)), ((), ())), preferr...]
    slice x86 -> x0, local copies, waits for them, and re-layouts: 25.7 us -> none  [the longest x60 23.8 us: shards(): lax.associative_scan(chain_pairs, (decays, drives), axis=0)]
    pad x32 -> x0, local copies, waits for them, and re-layouts: 21.8 us -> none  [shards(): lax.associative_scan(chain_pairs, (decays, drives), axis=0)]
    all_to_all x2 -> x0, starting transfers between devices: 21.1 us -> none  [from_everyone(): lax.all_to_all(jnp.broadcast_to(array[None], (count, *array.shape)), axis...]
    all_to_all x1 -> x0, blocking collectives: 15 us -> none  [sent_and_summed(): lax.all_to_all(parts, axis, split_axis=0, concat_axis=0, tiled=True)]
    add x35 -> x0, other arithmetic: 13 us -> none  [the longest x17 6.35 us: shards(): lax.associative_scan(chain_pairs, (decays, drives), axis=0)]
  transfers between devices with their start and end apart: 4 -> 0, of which waited for: 3 -> 0; matrix products, arithmetic and copies ran while one was open for 9% -> 0% of each run, Pallas kernels for 0% -> 0%
where the time goes in v1:
time: 95.7 us; the launch traced here: 95.6 us
  Pallas kernels  93.2 us (97%)
  local copies, waits for them, and re-layouts  2.3 us (2%)
    pallas_call x1, Pallas kernels, shards(): pl.pallas_call(functools.partial(kernel, ny, nz), out_shape=jax.ShapeDtyp...  93.2 us
    unnamed x1, local copies, waits for them, and re-layouts  2.3 us

profile of v1, /device:TPU:1, one launch (start us, length us, event | category | flops | bytes accessed | tf_op | source)
XLA Modules:
  0.0 95.6 jit_solution(9574767908584246748)
XLA Ops:
  0.0 93.2 %layer.1 = bf16[256,2048]{1,0:T(8,128)(2,1)} custom-call(bf16[256,2048]{1,0:T(8,128)(2,1)} %refs_0_.1, f32[1,2048]{1,0:T(1,128)} %bitcast.4, bf16[32,256]{1,0:T(8,128)(2,1)} %refs_2_.1, bf16[32,512]{1,0:T(8,128)(2,1)} %refs_3_.1, bf16[32,512]{1,0:T(8,128)(2,1)} %refs_4_.1, bf16[2,128,128]{2,1,0:T(8,128)(2,1)} %refs_5_.1, f32[1,256]{1,0:T(1,128)} %bitcast.7, ...), custom_call_target="tpu_custom_call" | custom-call | tf_op jit(solution)/shard_map/layer/pallas_call | solution.py:487
  93.3 2.3 %copy.17 = bf16[256,2048]{1,0:T(8,128)(2,1)} copy(bf16[256,2048]{1,0:T(8,128)(2,1)} %layer.1) | data formatting | bytes 2097152

commit v2 on v1

--- a/solution.py
+++ b/solution.py
@@ -18,17 +18,99 @@
 F32 = jnp.float32
 BF16 = jnp.bfloat16
 
-VALUE = 0
-GATES = (512, 896)
-POOLS = (768, 1152)
+GATE = 512
+POOL = 1024
 OUT = 1280
 PACKED = 2048
+PITCH = 72
 WINDOWS = (
-    ((0, 256), (512, 384), (1280, 256), (1536, 128)),
-    ((256, 256), (896, 384), (1664, 256), (1920, 128)),
+    ("value", 0, 0, 512, 32),
+    ("pool", 1, POOL, 256, 16),
+    ("gate0", 0, GATE, 256, None),
+    ("gate1", 1, GATE + 256, 256, None),
+    ("out0", 0, OUT, 256, None),
+    ("out1", 1, OUT + 256, 256, None),
+    ("out2", 0, OUT + 512, 128, None),
+    ("out3", 1, OUT + 640, 128, None),
 )
-STARTS = (0, 1, 4, 5)
-JOBS = len(STARTS)
+QUARTERS = 4
+LINK_RATE = 43e3
+HOP = 2.0
+
+
+def transfers_of(ny, nz, lines):
+    table, complete = {}, {}
+
+    def ring(head, axis, n, size, before):
+        reached = {0: tuple(before)}
+        for way in (1, -1):
+            last = tuple(before)
+            for step in range(1, n // 2 + 1):
+                key = (*head, way, step)
+                far = step == n // 2
+                table[key] = ((axis, way), size // 2 if far else size, last)
+                offset = n // 2 if far else -way * step
+                reached[offset] = reached.get(offset, ()) + (key,)
+                last = (key,)
+        return reached
+
+    def straight(head, axis, n, size):
+        reached = {0: ()}
+        for step in range(1, n // 2 + 1):
+            for way in (1, -1) if step < n // 2 else (1,):
+                key = (*head, way, step)
+                table[key] = ((axis, way), size * step, ())
+                reached[-way * step] = (key,)
+        return reached
+
+    for number, (name, order, _, width, rows) in enumerate(WINDOWS):
+        (p, np_), (q, nq) = (("y", ny), ("z", nz))[:: -1 if order else 1]
+        size = (rows or lines) * (LANES if rows else width) * 2
+        first = (straight if rows else ring)(
+            (number, 1, 0), p, np_, size, *(() if rows else ((),))
+        )
+        row = tuple(key for keys in first.values() for key in keys)
+        second = ring((number, 2, 0), q, nq, size * np_, row)
+        second[0] = row
+        keys = set(row).union(*second.values())
+        if rows:
+            for offset in sorted(second, key=lambda o: (abs(o), o)):
+                third = ring((number, 3, offset), "x", QUARTERS, size * np_, second[offset])
+                keys = keys.union(*(k for o, k in third.items() if o))
+        complete[name] = tuple(k for k in table if k in keys)
+    return table, complete
+
+
+def planned(transfers, tasks):
+    clock, free, at, order = 0.0, {}, {}, []
+    copies, pieces = dict(transfers), dict(tasks)
+    never = 1e9
+
+    def first_ready(table):
+        for key, entry in table.items():
+            if all(at.get(other, never) <= clock for other in entry[-1]):
+                return key
+        return None
+
+    while copies or pieces:
+        key = first_ready(copies)
+        if key is not None:
+            link, size, _ = copies.pop(key)
+            begin = max(clock, free.get(link, 0.0))
+            free[link] = begin + size / LINK_RATE
+            at[key] = free[link] + HOP
+            clock += 0.02
+            order.append(key)
+            continue
+        key = first_ready(pieces)
+        if key is not None:
+            cost, _ = pieces.pop(key)
+            clock += cost
+            at[key] = clock
+            order.append(key)
+            continue
+        clock = min(time for time in at.values() if time > clock)
+    return order
 
 
 def wrapped(index, count):
@@ -56,7 +138,7 @@
     (tok_in, gain_in, pool_in, gate_in, value_in, pmix_in, avg_in, taps_in, rmix_in, imix_in,
      lrate_in, shift_in, init_in, opool_in, ornn_in, out,
      w, tok, nrm, proj, aa, bb, acts, shift_t, gain, pmix, avg, taps, rmix, imix, lrate, shift,
-     init, bd, soft, ends_a, ends_b, enter, ybuf, zbuf, psend, precv, obuf,
+     init, bd, soft, ends_a, ends_b, enter, carried, ybuf, zbuf, psend, precv, own, obuf,
      local_sem, ring_send, ring_recv, pair_send, pair_recv, next_send, next_recv,
      y_send, y_recv, z_send, z_recv, part_send, part_recv, out_sem) = refs
     half, depth = tok_in.shape
@@ -64,7 +146,7 @@
     seg = rows // SEGMENTS
     rnn = lrate.shape[1]
     sp, tp = lax.axis_index("sp"), lax.axis_index("tp")
-    z, y = sp // ny, lax.rem(sp, ny)
+    z, y, x = sp // ny, lax.rem(sp, ny), lax.axis_index("fs")
     count = ny * nz
 
     def at_y(k):
@@ -77,19 +159,21 @@
         return pltpu.make_async_copy(src, dst, local_sem.at[k])
 
     mine = w.at[z, y]
+    lane = pl.multiple_of(x * LANES, LANES)
+    pool_lane = pl.multiple_of(x // 2 * LANES, LANES)
+    pool_lines = pl.ds(pl.multiple_of(lax.rem(x, 2) * 16, 16), 16)
     packing = [
-        local(0, value_in, mine.at[:, 0:512]),
-        local(1, gate_in.at[:, 0:256], mine.at[:, 512:768]),
-        local(2, pool_in.at[:, 0:128], mine.at[:, 768:896]),
-        local(3, gate_in.at[:, 256:512], mine.at[:, 896:1152]),
-        local(4, pool_in.at[:, 128:256], mine.at[:, 1152:1280]),
-        local(5, ornn_in, mine.at[:, 1280:1792]),
-        local(6, opool_in, mine.at[:, 1792:2048]),
+        local(0, value_in.at[:, pl.ds(lane, LANES)], mine.at[:, pl.ds(lane, LANES)]),
+        local(1, pool_in.at[pool_lines, pl.ds(pool_lane, LANES)],
+              mine.at[pool_lines, pl.ds(POOL + pool_lane, LANES)]),
+        local(2, gate_in, mine.at[:, GATE:POOL]),
+        local(3, ornn_in, mine.at[:, OUT:OUT + rnn]),
+        local(4, opool_in, mine.at[:, OUT + rnn:PACKED]),
     ]
     my_rows = pl.ds(pl.multiple_of(REACH + tp * half, REACH), half)
-    own_tokens = local(7, tok_in, tok.at[my_rows])
+    own_tokens = local(5, tok_in, tok.at[my_rows])
     small = [
-        local(8 + k, src, dst)
+        local(6 + k, src, dst)
         for k, (src, dst) in enumerate(
             [(gain_in, gain), (pmix_in, pmix), (avg_in, avg), (taps_in, taps), (rmix_in, rmix),
              (imix_in, imix), (lrate_in, lrate), (shift_in, shift), (init_in, init)]
@@ -104,80 +188,88 @@
     for peer in peers:
         pl.semaphore_signal(barrier, inc=1, device_id={"sp": peer}, device_id_type=MESH)
     pl.semaphore_signal(barrier, inc=1, device_id={"tp": 1 - tp}, device_id_type=MESH)
-    pl.semaphore_wait(barrier, len(peers) + 1)
+    for way in (1, -1):
+        pl.semaphore_signal(
+            barrier, inc=1, device_id={"fs": wrapped(x + way, QUARTERS)}, device_id_type=MESH
+        )
+    for copy in packing:
+        copy.wait()
+    pl.semaphore_wait(barrier, len(peers) + 3)
 
     pair = pltpu.make_async_remote_copy(
         src_ref=tok_in, dst_ref=tok.at[my_rows], send_sem=pair_send, recv_sem=pair_recv,
         device_id={"tp": 1 - tp}, device_id_type=MESH,
     )
-    pair.start()
     halo = pltpu.make_async_remote_copy(
         src_ref=tok.at[pl.ds(rows, REACH)], dst_ref=tok.at[pl.ds(0, REACH)],
         send_sem=next_send, recv_sem=next_recv,
         device_id={"sp": wrapped(sp + 1, count)}, device_id_type=MESH,
     )
 
-    sizes = ((ny, nz), (nz, ny))
-    homes = ((y, z), (z, y))
-
-    def hops(color, job, phase, way):
-        n = sizes[color][phase]
-        return n // 2 if (way + job + color) % 2 == 0 else (n - 1) // 2
-
-    def block(color, job, phase, origin):
-        first, width = WINDOWS[color][job]
-        cols = pl.ds(first, width)
-        if color == 0:
-            return w.at[z, origin, :, cols] if phase == 0 else w.at[origin, :, :, cols]
-        return w.at[origin, y, :, cols] if phase == 0 else w.at[:, origin, :, cols]
-
-    def ring(color, job, phase, way, step, arriving):
-        n = sizes[color][phase]
-        home = homes[color][phase]
-        back = step + 1 if arriving else step
-        origin = wrapped(home - back if way == 0 else home + back, n)
-        on_y = (color == 0) == (phase == 0)
-        ahead = 1 if way == 0 else -1
-        ref = block(color, job, phase, origin)
+    table, complete = transfers_of(ny, nz, w.shape[2])
+    places = {key: k for k, key in enumerate(table)}
+    groups = {}
+    for key in table:
+        groups.setdefault(key[:3], len(groups))
+    sizes = {"y": ny, "z": nz, "x": QUARTERS}
+    homes = {"y": y, "z": z, "x": x}
+
+    def region(number, phase, offset, origin, half):
+        _, order, first, width, rows = WINDOWS[number]
+        p, q = ("z", "y") if order else ("y", "z")
+        at = {p: slice(None), q: homes[q]}
+        if phase == 1:
+            at[p] = wrapped(homes[p] + origin, sizes[p])
+        else:
+            at[q] = wrapped(homes[q] + (origin if phase == 2 else offset), sizes[q])
+            if half is not None:
+                at[p] = pl.ds(half * (sizes[p] // 2), sizes[p] // 2)
+        lines, cols = slice(None), pl.ds(first, width)
+        if rows:
+            part = wrapped(x + origin, QUARTERS) if phase == 3 else x
+            if rows < w.shape[2]:
+                lines = pl.ds(pl.multiple_of(lax.rem(part, 2) * rows, rows), rows)
+                part = part // 2
+            cols = pl.ds(pl.multiple_of(first + part * LANES, LANES), LANES)
+        elif phase == 1 and half is not None:
+            lines = pl.ds(half * 16, 16)
+        return w.at[at["z"], at["y"], lines, cols]
+
+    def gather_copy(key, arriving):
+        number, phase, offset, way, step = key
+        _, order, _, _, rows = WINDOWS[number]
+        straight = rows and phase == 1
+        axis = table[key][0][0]
+        far = step == sizes[axis] // 2 and not straight
+        origin = -way * (step if arriving else 0 if straight else step - 1)
+        ref = region(number, phase, offset, origin, (1 - way) // 2 if far else None)
+        ahead = way * (step if straight else 1)
+        target = {
+            "y": lambda: {"sp": at_y(ahead)},
+            "z": lambda: {"sp": at_z(ahead)},
+            "x": lambda: {"fs": wrapped(x + ahead, QUARTERS)},
+        }[axis]()
         return pltpu.make_async_remote_copy(
-            src_ref=ref, dst_ref=ref,
-            send_sem=ring_send.at[color, job, phase, way, step],
-            recv_sem=ring_recv.at[color, job, phase, way, step],
-            device_id={"sp": at_y(ahead) if on_y else at_z(ahead)}, device_id_type=MESH,
-        )
-
-    def steps_of(color, job):
-        result = []
-        for phase in (0, 1):
-            for step in range(max(hops(color, job, phase, 0), hops(color, job, phase, 1))):
-                result.append([
-                    (color, job, phase, way, step) for way in (0, 1)
-                    if step < hops(color, job, phase, way)
-                ])
-        return result
-
-    plans = {(c, j): steps_of(c, j) for c in (0, 1) for j in range(JOBS)}
-    started = []
-
-    def advance(color, job, at):
-        plan = plans[color, job]
-        if 0 < at <= len(plan):
-            for key in plan[at - 1]:
-                ring(*key, True).wait_recv()
-        if 0 <= at < len(plan):
-            for key in plan[at]:
-                ring(*key, False).start()
-                started.append(key)
-
-    def round_of(r):
-        if r == 0:
-            packing[0].wait()
-        if r == STARTS[1]:
-            for copy in packing[1:]:
-                copy.wait()
-        for job in range(JOBS):
-            for color in (0, 1):
-                advance(color, job, r - STARTS[job])
+            src_ref=ref, dst_ref=ref, send_sem=ring_send.at[groups[key[:3]]],
+            recv_sem=ring_recv.at[places[key]], device_id=target, device_id_type=MESH,
+        )
+
+    def all_sent(group):
+        number, phase, _ = group
+        _, order, first, width, rows = WINDOWS[number]
+        lines = slice(0, rows or w.shape[2])
+        cols = slice(first, first + (LANES if rows else width))
+        if phase == 3:
+            cols = slice(0, (QUARTERS - 1) * LANES)
+            ref = w.at[:, 0, lines, cols] if order else w.at[0, :, lines, cols]
+        elif (phase == 1) == (order == 0):
+            lead = slice(0, ny - 1)
+            ref = w.at[0 if phase == 1 else slice(None), lead, lines, cols]
+        else:
+            lead = slice(0, nz - 1)
+            ref = w.at[lead, 0 if phase == 1 else slice(None), lines, cols]
+        sem = ring_send.at[groups[group]]
+        pltpu.make_async_copy(ref, ref, sem).wait()
 
     def prepare():
         for copy in small:
@@ -202,7 +294,7 @@
             keep = jnp.where(jnp.logical_and(i == 0, sp == 0), 0.0, 1.0)
             nrm[at, :] = (x * lax.rsqrt(mean + EPSILON) * gain[...] * keep).astype(BF16)
             return carry
-        lax.fori_loop(first, last, body, 0)
+        lax.fori_loop(first, last, body, 0, unroll=3)
 
     def project(first, last):
         def body(n, carry):
@@ -213,7 +305,7 @@
             return carry
         lax.fori_loop(first, last, body, 0)
 
-    def gates():
+    def gates(begin, end):
         low = lax.broadcasted_iota(jnp.int32, (seg, LANES), 1) < HEAD
 
         def body(i, carry):
@@ -233,18 +325,19 @@
                     low, shift_t[at, 2 * k:2 * k + 1], shift_t[at, 2 * k + 1:2 * k + 2]
                 )
                 log_decay = rate * soft[0:1, cols] + shifts
-                aa[k, at, :] = jnp.exp(log_decay)
-                bb[k, at, :] = (
+                put = pl.ds(pl.multiple_of(i * PITCH, 8), seg)
+                aa[k, put, :] = jnp.exp(log_decay)
+                bb[k, put, :] = (
                     jnp.sqrt(one_minus_exp(2.0 * log_decay)) * entry * conv.astype(F32)
                 )
             return carry
-        lax.fori_loop(0, SEGMENTS, body, 0)
+        lax.fori_loop(begin, end, body, 0)
 
     def scan():
         tiles = range(rnn // LANES)
 
         def body(j, carry):
-            at = pl.ds(j, SEGMENTS, stride=seg)
+            at = pl.ds(j, SEGMENTS, stride=PITCH)
             result = []
             for k in tiles:
                 decay, state = carry[k]
@@ -289,13 +382,16 @@
             whole = (whole[0] * a, a * whole[1] + b)
         return whole, before
 
+    def turned(first):
+        return pl.ds(pl.multiple_of(lax.rem(first + (1 - tp) * half, rows), REACH), seg)
+
     def pool():
         def body(i, carry):
             first = pl.multiple_of(i * seg, seg)
-            at = pl.ds(first, seg)
+            at = turned(first)
             place = sp * rows + first + lax.broadcasted_iota(jnp.int32, (seg, LANES), 0)
             for g in (0, 1):
-                x = proj[pl.ds(first, seg + REACH), POOLS[g]:POOLS[g] + LANES]
+                x = proj[pl.ds(first, seg + REACH), POOL + g * LANES:POOL + (g + 1) * LANES]
                 near = x + pltpu.roll(x, 1, 0)
                 if g == 1:
                     near = near + pltpu.roll(near, 2, 0)
@@ -319,27 +415,35 @@
 
         def body(i, carry):
             at = pl.ds(pl.multiple_of(REACH + i * seg, REACH), seg)
-            for g in (0, 1):
-                cols = slice(GATES[g], GATES[g] + 256)
-                x = proj[at, cols]
-                proj[at, cols] = x * (
-                    0.5 * (1.0 + jnp.tanh(scale * (x + 0.044715 * (x * x * x))))
-                )
+            cols = slice(GATE, POOL)
+            v = proj[at, cols]
+            proj[at, cols] = v * (0.5 * (1.0 + jnp.tanh(scale * (v + 0.044715 * (v * v * v)))))
             return carry
         lax.fori_loop(0, SEGMENTS, body, 0)
 
-    def finish(carried):
+    def carry_in():
+        _, rows_before = chained(zbuf, nz, z)
+        _, in_row = chained(ybuf, ny, y)
+        entry = rows_before[0] * init[...] + rows_before[1]
+        carried[...] = in_row[0] * entry + in_row[1]
+
+    def row_total():
+        whole, _ = chained(ybuf, ny, y)
+        zbuf[z, :, 0:rnn] = whole[0]
+        zbuf[z, :, rnn:] = whole[1]
+
+    def finish():
         def body(i, carry):
             first = pl.multiple_of(i * seg, seg)
-            at = pl.ds(first, seg)
-            begin = enter[i, :, 0:rnn] * carried + enter[i, :, rnn:]
+            at = pl.ds(pl.multiple_of(i * PITCH, 8), seg)
+            put = turned(first)
+            begin = enter[i, :, 0:rnn] * carried[...] + enter[i, :, rnn:]
             for k in range(rnn // LANES):
                 cols = slice(k * LANES, (k + 1) * LANES)
                 state = bb[k, at, :] + aa[k, at, :] * begin[:, cols]
-                column = GATES[k // 2] + k % 2 * LANES
                 gate = proj[pl.ds(pl.multiple_of(REACH + first, REACH), seg),
-                            column:column + LANES]
-                acts[at, cols] = (gate * state).astype(BF16)
+                            GATE + k * LANES:GATE + (k + 1) * LANES]
+                acts[put, cols] = (gate * state).astype(BF16)
             return carry
         lax.fori_loop(0, SEGMENTS, body, 0)
 
@@ -351,12 +455,17 @@
             recv_sem=part_recv.at[n], device_id={"tp": 1 - tp}, device_id_type=MESH,
         )
 
-    def product(side, n):
-        at = pl.ds(pl.multiple_of(side * half, REACH), half)
-        weight = w[n, :, :, OUT:PACKED].reshape(features, PACKED - OUT)
-        return lax.dot_general(
-            acts[at, :], weight, (((1,), (1,)), ((), ())), preferred_element_type=F32
-        )
+    def products():
+        def body(n, carry):
+            weight = w[n, :, :, OUT:PACKED].reshape(features, PACKED - OUT)
+            result = lax.dot_general(
+                acts[...], weight, (((1,), (1,)), ((), ())), preferred_element_type=F32
+            )
+            psend[n] = result[:half].astype(BF16)
+            part_copy(n).start()
+            own[n] = result[half:]
+            return carry
+        lax.fori_loop(0, nz, body, 0)
 
     def out_copy(n):
         return pltpu.make_async_copy(
@@ -364,70 +473,89 @@
             out_sem.at[n],
         )
 
-    round_of(0)
-    own_tokens.wait()
-    pair.wait_recv()
-    halo.start()
-    round_of(1)
-    prepare()
-    round_of(2)
-    halo.wait_recv()
-    normalize(0, 17)
-    round_of(3)
-    normalize(17, (rows + REACH) // REACH)
-    plan_len = max(len(p) for p in plans.values())
-    for r in range(4, plan_len + 1):
-        round_of(r)
-    project(0, 2)
-    round_of(plan_len + 1)
-    gates()
-    round_of(plan_len + 2)
-    scan()
-    for k in range(1, ny):
-        y_copy(k, False).start()
-    round_of(plan_len + 3)
-    project(2, 5)
-    for k in range(1, ny):
-        y_copy(k, True).wait_recv()
-    whole, in_row = chained(ybuf, ny, y)
-    zbuf[z, :, 0:rnn] = whole[0]
-    zbuf[z, :, rnn:] = whole[1]
-    for k in range(1, nz):
-        z_copy(k, False).start()
-    round_of(plan_len + 4)
-    pool()
-    gelu()
-    round_of(plan_len + 5)
-    for k in range(1, nz):
-        z_copy(k, True).wait_recv()
-    _, rows_before = chained(zbuf, nz, z)
-    carried = in_row[0] * (rows_before[0] * init[...] + rows_before[1]) + in_row[1]
-    finish(carried)
-
-    def to_partner(n, carry):
-        psend[n] = product(1 - tp, n).astype(BF16)
-        part_copy(n).start()
-        return carry
-
-    lax.fori_loop(0, nz, to_partner, 0)
-
-    def for_me(n, carry):
-        own = product(tp, n)
-        part_copy(n).wait_recv()
-        obuf[n] = (own + precv[n].astype(F32)).astype(BF16)
-        out_copy(n).start()
-        return carry
-
-    lax.fori_loop(0, nz, for_me, 0)
-
-    for key in started:
-        ring(*key, False).wait_send()
-    pair.wait_send()
-    halo.wait_send()
-    for k in range(1, ny):
-        y_copy(k, False).wait_send()
-    for k in range(1, nz):
-        z_copy(k, False).wait_send()
+    def totals():
+        def body(n, carry):
+            part_copy(n).wait_recv()
+            obuf[n] = (own[n] + precv[n].astype(F32)).astype(BF16)
+            out_copy(n).start()
+            return carry
+        lax.fori_loop(0, nz, body, 0)
+
+    copies = {"pair": (None, 0, ()), "halo": (None, 0, ("pair", "own"))}
+    copies.update({"y_sums": (None, 0, ("scan",)), "z_sums": (None, 0, ("row_total",))})
+    copies.update(table)
+    blocks = (rows + REACH) // REACH
+    cuts = [blocks * k // 4 // 3 * 3 for k in range(4)] + [blocks]
+    normed = tuple(f"norm{k}" for k in range(4))
+    pieces = {"own": (0.0, own_tokens.wait, ()), "prepare": (0.3, prepare, ())}
+    for k in range(4):
+        pieces[normed[k]] = (
+            0.8, functools.partial(normalize, cuts[k], cuts[k + 1]), ("halo",)
+        )
+    for k in range(2):
+        pieces[f"value{k}"] = (
+            0.8, functools.partial(project, k, k + 1), complete["value"] + normed
+        )
+    for k in range(4):
+        pieces[f"gates{k}"] = (
+            0.8, functools.partial(gates, 2 * k, 2 * k + 2), ("value0", "value1", "prepare")
+        )
+    pieces["scan"] = (1.5, scan, tuple(f"gates{k}" for k in range(4)))
+    pieces["row_total"] = (0.1, row_total, ("y_sums",))
+    pieces["carry_in"] = (0.1, carry_in, ("z_sums",))
+    for k in range(2):
+        pieces[f"gate{k}"] = (
+            0.8, functools.partial(project, 2 + k, 3 + k), complete[f"gate{k}"] + normed
+        )
+    pieces["project_pool"] = (0.8, functools.partial(project, 4, 5), complete["pool"] + normed)
+    pieces["gelu"] = (0.4, gelu, ("gate0", "gate1"))
+    pieces["pool"] = (1.4, pool, ("project_pool", "prepare"))
+    pieces["finish"] = (0.3, finish, ("carry_in", "gelu"))
+    outs = sum((complete[f"out{k}"] for k in range(4)), ())
+    pieces["products"] = (2.5, products, ("finish", "pool") + outs)
+    pieces["totals"] = (1.5, totals, ("products",))
+
+    def y_all(arriving):
+        return [y_copy(k, arriving) for k in range(1, ny)]
+
+    def z_all(arriving):
+        return [z_copy(k, arriving) for k in range(1, nz)]
+
+    def started(key, arriving):
+        if key == "pair":
+            return [pair]
+        if key == "halo":
+            return [halo]
+        if key == "y_sums":
+            return y_all(arriving)
+        if key == "z_sums":
+            return z_all(arriving)
+        return [gather_copy(key, arriving)]
+
+    waited = set()
+
+    def settle(keys):
+        for key in keys:
+            if key in copies and key not in waited:
+                waited.add(key)
+                for copy in started(key, True):
+                    copy.wait_recv()
+
+    for key in planned(copies, {k: (v[0], v[2]) for k, v in pieces.items()}):
+        if key in copies:
+            settle(copies[key][-1])
+            for copy in started(key, False):
+                copy.start()
+        else:
+            settle(pieces[key][-1])
+            pieces[key][1]()
+    settle(copies)
+
+    for group in groups:
+        all_sent(group)
+    for key in ("pair", "halo", "y_sums", "z_sums"):
+        for copy in started(key, False):
+            copy.wait_send()
 
     def ended(n, carry):
         part_copy(n).wait_send()
@@ -445,7 +573,7 @@
     rnn = log_rate.shape[0]
     lines = pool_in.shape[0]
     features = ny * lines
-    steps = max(ny, nz) // 2
+    table, _ = transfers_of(ny, nz, lines)
     dma = pltpu.SemaphoreType.DMA
     vmem = pltpu.VMEM
     scratch = [
@@ -453,8 +581,8 @@
         vmem((rows + REACH, depth), BF16),
         vmem((rows + REACH, depth), BF16),
         vmem((rows + REACH, OUT), F32),
-        vmem((rnn // LANES, rows, LANES), F32),
-        vmem((rnn // LANES, rows, LANES), F32),
+        vmem((rnn // LANES, SEGMENTS * PITCH, LANES), F32),
+        vmem((rnn // LANES, SEGMENTS * PITCH, LANES), F32),
         vmem((rows, PACKED - OUT), BF16),
         vmem((rows, rnn // HEAD), F32),
         vmem((1, depth), F32),
@@ -471,14 +599,16 @@
         vmem((SEGMENTS, rnn), F32),
         vmem((SEGMENTS, rnn), F32),
         vmem((SEGMENTS, 1, 2 * rnn), F32),
+        vmem((1, rnn), F32),
         vmem((ny, 1, 2 * rnn), F32),
         vmem((nz, 1, 2 * rnn), F32),
         vmem((nz, half, features), BF16),
         vmem((nz, half, features), BF16),
+        vmem((nz, half, features), F32),
         vmem((nz, half, features), BF16),
-        dma((17,)),
-        dma((2, JOBS, 2, 2, steps)),
-        dma((2, JOBS, 2, 2, steps)),
+        dma((15,)),
+        dma((len({key[:3] for key in table}),)),
+        dma((len(table),)),
         dma, dma, dma, dma,
         dma((ny,)), dma((ny,)), dma((nz,)), dma((nz,)),
         dma((nz,)), dma((nz,)), dma((nz,)),

time: 95.7 us -> 78.9 us (0.82)
  Pallas kernels: 93.2 us -> 76.5 us
    pallas_call x1, Pallas kernels: 93.2 us -> 76.5 us  [shards(): pl.pallas_call(functools.partial(kernel, ny, nz), out_shape=jax.ShapeDtyp...]
where the time goes in v2:
time: 78.9 us; the launch traced here: 78.8 us
  Pallas kernels  76.5 us (97%)
  local copies, waits for them, and re-layouts  2.3 us (3%)
    pallas_call x1, Pallas kernels, shards(): pl.pallas_call(functools.partial(kernel, ny, nz), out_shape=jax.ShapeDtyp...  76.5 us
    unnamed x1, local copies, waits for them, and re-layouts  2.3 us

profile of v2, /device:TPU:1, one launch (start us, length us, event | category | flops | bytes accessed | tf_op | source)
XLA Modules:
  0.0 78.8 jit_solution(11357154618732609442)
XLA Ops:
  0.0 76.5 %layer.1 = bf16[256,2048]{1,0:T(8,128)(2,1)} custom-call(bf16[256,2048]{1,0:T(8,128)(2,1)} %refs_0_.1, f32[1,2048]{1,0:T(1,128)} %bitcast.4, bf16[32,256]{1,0:T(8,128)(2,1)} %refs_2_.1, bf16[32,512]{1,0:T(8,128)(2,1)} %refs_3_.1, bf16[32,512]{1,0:T(8,128)(2,1)} %refs_4_.1, bf16[2,128,128]{2,1,0:T(8,128)(2,1)} %refs_5_.1, f32[1,256]{1,0:T(1,128)} %bitcast.7, ...), custom_call_target="tpu_custom_call" | custom-call | tf_op jit(solution)/shard_map/layer/pallas_call | solution.py:617
  76.5 2.3 %copy.17 = bf16[256,2048]{1,0:T(8,128)(2,1)} copy(bf16[256,2048]{1,0:T(8,128)(2,1)} %layer.1) | data formatting | bytes 2097152

commit v3 on v2

--- a/solution.py
+++ b/solution.py
@@ -18,24 +18,27 @@
 F32 = jnp.float32
 BF16 = jnp.bfloat16
 
+VALUE = 0
 GATE = 512
 POOL = 1024
 OUT = 1280
 PACKED = 2048
 PITCH = 72
 WINDOWS = (
-    ("value", 0, 0, 512, 32),
-    ("pool", 1, POOL, 256, 16),
-    ("gate0", 0, GATE, 256, None),
-    ("gate1", 1, GATE + 256, 256, None),
-    ("out0", 0, OUT, 256, None),
-    ("out1", 1, OUT + 256, 256, None),
-    ("out2", 0, OUT + 512, 128, None),
-    ("out3", 1, OUT + 640, 128, None),
+    ("value", 0, 0, 256, True, None),
+    ("gate", 0, GATE, 256, True, 1),
+    ("gate", 1, GATE + 384, 128, False, None),
+    ("gate", 0, GATE + 256, 128, False, 1),
+    ("value", 1, 256, 256, True, None),
+    ("pool", 1, POOL, 256, True, 2),
+    ("out", 0, OUT, 128, False, 3),
+    ("out", 0, OUT + 128, 256, False, 2),
+    ("out", 1, OUT + 384, 256, False, 3),
+    ("out", 1, OUT + 640, 128, False, None),
 )
-QUARTERS = 4
-LINK_RATE = 43e3
-HOP = 2.0
+X_RING = 4
+LINK_RATE = 40e3
+HOP = 2.2
 
 
 def transfers_of(ny, nz, lines):
@@ -63,22 +66,43 @@
                 reached[-way * step] = (key,)
         return reached
 
-    for number, (name, order, _, width, rows) in enumerate(WINDOWS):
+    for number, (name, order, _, width, shared, hold) in enumerate(WINDOWS):
         (p, np_), (q, nq) = (("y", ny), ("z", nz))[:: -1 if order else 1]
-        size = (rows or lines) * (LANES if rows else width) * 2
-        first = (straight if rows else ring)(
-            (number, 1, 0), p, np_, size, *(() if rows else ((),))
+        size = lines * (width // 2 if shared else width) * 2
+        first = straight((number, 1, 0), p, np_, size) if shared else ring(
+            (number, 1, 0), p, np_, size, ()
         )
         row = tuple(key for keys in first.values() for key in keys)
         second = ring((number, 2, 0), q, nq, size * np_, row)
         second[0] = row
+        if hold is not None:
+            leader = [w[:2] for w in WINDOWS].index(("value", order))
+            for way in (1, -1):
+                link, size_, before = table[number, 2, 0, way, 1]
+                sent = ("sent", (leader, 2, 0, way, min(hold, nq // 2)))
+                table[number, 2, 0, way, 1] = (link, size_, before + (sent,))
         keys = set(row).union(*second.values())
-        if rows:
+        if shared:
             for offset in sorted(second, key=lambda o: (abs(o), o)):
-                third = ring((number, 3, offset), "x", QUARTERS, size * np_, second[offset])
-                keys = keys.union(*(k for o, k in third.items() if o))
-        complete[name] = tuple(k for k in table if k in keys)
+                for way in (1, -1):
+                    key = (number, 3, offset, way, 1)
+                    table[key] = (("x", way), size * np_ // 2, second[offset])
+                    keys.add(key)
+        complete[name] = complete.get(name, ()) + tuple(k for k in table if k in keys)
     return table, complete
+
+
+def semaphores_of(table, ny, nz):
+    sends, recvs = {}, {}
+    for key in table:
+        number, phase, _, _, step = key
+        order, shared = WINDOWS[number][1], WINDOWS[number][4]
+        n = (ny, nz)[(phase - 1) ^ order] if phase < 3 else 0
+        together = phase == 3 or (shared and phase == 1) or step == n // 2
+        recvs[key] = (number, phase, "all" if phase == 3 or (shared and phase == 1) else "far") \
+            if together else key
+        sends[key] = (number, phase)
+    return sends, recvs
 
 
 def planned(transfers, tasks):
@@ -96,9 +120,10 @@
         key = first_ready(copies)
         if key is not None:
             link, size, _ = copies.pop(key)
-            begin = max(clock, free.get(link, 0.0))
+            begin = max(clock, free.get(link, 0.0)) if link else clock
             free[link] = begin + size / LINK_RATE
-            at[key] = free[link] + HOP
+            at[key] = free[link] + HOP * (1 if link else 2)
+            at["sent", key] = clock
             clock += 0.02
             order.append(key)
             continue
@@ -127,11 +152,12 @@
     return jnp.maximum(v, 0.0) + 2.0 * s * total
 
 
-def one_minus_exp(y):
-    series = jnp.full_like(y, 1.0)
-    for k in (9, 8, 7, 6, 5, 4, 3, 2):
-        series = 1.0 + series * y * (1.0 / k)
-    return jnp.where(y > -0.6, -y * series, 1.0 - jnp.exp(y))
+def one_minus_square(a, x):
+    v = 2.0 * x
+    series = jnp.full_like(v, 1.0 / 720.0)
+    for k in (120.0, 24.0, 6.0, 2.0, 1.0):
+        series = series * v + 1.0 / k
+    return jnp.where(v > -0.25, -v * series, 1.0 - a * a)
 
 
 def kernel(ny, nz, *refs):
@@ -140,7 +166,7 @@
      w, tok, nrm, proj, aa, bb, acts, shift_t, gain, pmix, avg, taps, rmix, imix, lrate, shift,
      init, bd, soft, ends_a, ends_b, enter, carried, ybuf, zbuf, psend, precv, own, obuf,
      local_sem, ring_send, ring_recv, pair_send, pair_recv, next_send, next_recv,
-     y_send, y_recv, z_send, z_recv, part_send, part_recv, out_sem) = refs
+     y_sem, z_sem, part_send, part_recv, out_sem) = refs
     half, depth = tok_in.shape
     rows = 2 * half
     seg = rows // SEGMENTS
@@ -159,21 +185,24 @@
         return pltpu.make_async_copy(src, dst, local_sem.at[k])
 
     mine = w.at[z, y]
-    lane = pl.multiple_of(x * LANES, LANES)
-    pool_lane = pl.multiple_of(x // 2 * LANES, LANES)
-    pool_lines = pl.ds(pl.multiple_of(lax.rem(x, 2) * 16, 16), 16)
-    packing = [
-        local(0, value_in.at[:, pl.ds(lane, LANES)], mine.at[:, pl.ds(lane, LANES)]),
-        local(1, pool_in.at[pool_lines, pl.ds(pool_lane, LANES)],
-              mine.at[pool_lines, pl.ds(POOL + pool_lane, LANES)]),
-        local(2, gate_in, mine.at[:, GATE:POOL]),
-        local(3, ornn_in, mine.at[:, OUT:OUT + rnn]),
-        local(4, opool_in, mine.at[:, OUT + rnn:PACKED]),
-    ]
+    parity = lax.rem(x, 2)
+    sources = {"value": (value_in, 0), "gate": (gate_in, GATE), "pool": (pool_in, POOL)}
+    packing = []
+    for name, _, first, width, shared, _ in WINDOWS:
+        if name in sources:
+            src, base = sources[name]
+            if shared:
+                skip, width = pl.multiple_of(parity * LANES, LANES), width // 2
+                cols, from_ = pl.ds(first + skip, width), pl.ds(first - base + skip, width)
+            else:
+                cols, from_ = pl.ds(first, width), pl.ds(first - base, width)
+            packing.append(local(len(packing), src.at[:, from_], mine.at[:, cols]))
+    packing.append(local(len(packing), ornn_in, mine.at[:, OUT:OUT + rnn]))
+    packing.append(local(len(packing), opool_in, mine.at[:, OUT + rnn:PACKED]))
     my_rows = pl.ds(pl.multiple_of(REACH + tp * half, REACH), half)
-    own_tokens = local(5, tok_in, tok.at[my_rows])
+    own_tokens = local(8, tok_in, tok.at[my_rows])
     small = [
-        local(6 + k, src, dst)
+        local(9 + k, src, dst)
         for k, (src, dst) in enumerate(
             [(gain_in, gain), (pmix_in, pmix), (avg_in, avg), (taps_in, taps), (rmix_in, rmix),
              (imix_in, imix), (lrate_in, lrate), (shift_in, shift), (init_in, init)]
@@ -190,7 +219,7 @@
     pl.semaphore_signal(barrier, inc=1, device_id={"tp": 1 - tp}, device_id_type=MESH)
     for way in (1, -1):
         pl.semaphore_signal(
-            barrier, inc=1, device_id={"fs": wrapped(x + way, QUARTERS)}, device_id_type=MESH
+            barrier, inc=1, device_id={"fs": wrapped(x + way, X_RING)}, device_id_type=MESH
         )
     for copy in packing:
         copy.wait()
@@ -207,69 +236,67 @@
     )
 
     table, complete = transfers_of(ny, nz, w.shape[2])
-    places = {key: k for k, key in enumerate(table)}
-    groups = {}
-    for key in table:
-        groups.setdefault(key[:3], len(groups))
-    sizes = {"y": ny, "z": nz, "x": QUARTERS}
-    homes = {"y": y, "z": z, "x": x}
-
-    def region(number, phase, offset, origin, half):
-        _, order, first, width, rows = WINDOWS[number]
+    sends, recvs = semaphores_of(table, ny, nz)
+    send_at = {group: k for k, group in enumerate(dict.fromkeys(sends.values()))}
+    recv_at = {group: k for k, group in enumerate(dict.fromkeys(recvs.values()))}
+    sizes = {"y": ny, "z": nz}
+    homes = {"y": y, "z": z}
+
+    def region(key, arriving):
+        number, phase, offset, way, step = key
+        _, order, first, width, shared, _ = WINDOWS[number]
         p, q = ("z", "y") if order else ("y", "z")
+        straight = shared and phase == 1
+        far = phase == 3 or (step == sizes[p if phase == 1 else q] // 2 and not straight)
+        half = (1 - way) // 2
+        origin = -way * (step if arriving else 0 if straight else step - 1)
         at = {p: slice(None), q: homes[q]}
+        lines, cols = slice(None), pl.ds(first, width)
         if phase == 1:
             at[p] = wrapped(homes[p] + origin, sizes[p])
+            if far:
+                lines = pl.ds(half * 16, 16)
         else:
             at[q] = wrapped(homes[q] + (origin if phase == 2 else offset), sizes[q])
-            if half is not None:
+            if far:
                 at[p] = pl.ds(half * (sizes[p] // 2), sizes[p] // 2)
-        lines, cols = slice(None), pl.ds(first, width)
-        if rows:
-            part = wrapped(x + origin, QUARTERS) if phase == 3 else x
-            if rows < w.shape[2]:
-                lines = pl.ds(pl.multiple_of(lax.rem(part, 2) * rows, rows), rows)
-                part = part // 2
-            cols = pl.ds(pl.multiple_of(first + part * LANES, LANES), LANES)
-        elif phase == 1 and half is not None:
-            lines = pl.ds(half * 16, 16)
+        if shared:
+            side = 1 - parity if phase == 3 and arriving else parity
+            cols = pl.ds(pl.multiple_of(first + side * LANES, LANES), LANES)
         return w.at[at["z"], at["y"], lines, cols]
 
-    def gather_copy(key, arriving):
-        number, phase, offset, way, step = key
-        _, order, _, _, rows = WINDOWS[number]
-        straight = rows and phase == 1
+    def gather_copy(key):
+        number, phase, _, way, step = key
         axis = table[key][0][0]
-        far = step == sizes[axis] // 2 and not straight
-        origin = -way * (step if arriving else 0 if straight else step - 1)
-        ref = region(number, phase, offset, origin, (1 - way) // 2 if far else None)
-        ahead = way * (step if straight else 1)
+        ahead = way * (step if WINDOWS[number][4] and phase == 1 else 1)
         target = {
             "y": lambda: {"sp": at_y(ahead)},
             "z": lambda: {"sp": at_z(ahead)},
-            "x": lambda: {"fs": wrapped(x + ahead, QUARTERS)},
+            "x": lambda: {"fs": wrapped(x + ahead, X_RING)},
         }[axis]()
+        ref = region(key, False)
         return pltpu.make_async_remote_copy(
-            src_ref=ref, dst_ref=ref, send_sem=ring_send.at[groups[key[:3]]],
-            recv_sem=ring_recv.at[places[key]], device_id=target, device_id_type=MESH,
-        )
-
-    def all_sent(group):
-        number, phase, _ = group
-        _, order, first, width, rows = WINDOWS[number]
-        lines = slice(0, rows or w.shape[2])
-        cols = slice(first, first + (LANES if rows else width))
+            src_ref=ref, dst_ref=ref, send_sem=ring_send.at[send_at[sends[key]]],
+            recv_sem=ring_recv.at[recv_at[recvs[key]]], device_id=target, device_id_type=MESH,
+        )
+
+    def block_of(number, phase, what):
+        _, order, first, width, shared, _ = WINDOWS[number]
+        cols = slice(first, first + (LANES if shared else width))
         if phase == 3:
-            cols = slice(0, (QUARTERS - 1) * LANES)
-            ref = w.at[:, 0, lines, cols] if order else w.at[0, :, lines, cols]
-        elif (phase == 1) == (order == 0):
-            lead = slice(0, ny - 1)
-            ref = w.at[0 if phase == 1 else slice(None), lead, lines, cols]
-        else:
-            lead = slice(0, nz - 1)
-            ref = w.at[lead, 0 if phase == 1 else slice(None), lines, cols]
-        sem = ring_send.at[groups[group]]
+            return w.at[:, :, :, cols]
+        along_y = (phase == 1) == (order == 0)
+        size = (ny if along_y else nz) - 1
+        other = slice(None) if phase == 2 else 0
+        some = slice(0, size) if what == "all" else 0
+        return w.at[other, some, :, cols] if along_y else w.at[some, other, :, cols]
+
+    def wait_for(ref, sem):
         pltpu.make_async_copy(ref, ref, sem).wait()
+
+    def arrived(group):
+        sem = ring_recv.at[recv_at[group]]
+        wait_for(block_of(*group) if len(group) == 3 else region(group, True), sem)
 
     def prepare():
         for copy in small:
@@ -296,14 +323,10 @@
             return carry
         lax.fori_loop(first, last, body, 0, unroll=3)
 
-    def project(first, last):
-        def body(n, carry):
-            cols = pl.ds(pl.multiple_of(n * 256, 256), 256)
-            weight = w[:, :, :, cols].reshape(depth, 256)
-            result = jnp.dot(nrm[...], weight, preferred_element_type=F32)
-            proj[:, cols] = result.astype(BF16).astype(F32)
-            return carry
-        lax.fori_loop(first, last, body, 0)
+    def project(first, width):
+        weight = w[:, :, :, first:first + width].reshape(depth, width)
+        result = jnp.dot(nrm[...], weight, preferred_element_type=F32)
+        proj[:, first:first + width] = result.astype(BF16).astype(F32)
 
     def gates(begin, end):
         low = lax.broadcasted_iota(jnp.int32, (seg, LANES), 1) < HEAD
@@ -326,9 +349,10 @@
                 )
                 log_decay = rate * soft[0:1, cols] + shifts
                 put = pl.ds(pl.multiple_of(i * PITCH, 8), seg)
-                aa[k, put, :] = jnp.exp(log_decay)
+                decay = jnp.exp(log_decay)
+                aa[k, put, :] = decay
                 bb[k, put, :] = (
-                    jnp.sqrt(one_minus_exp(2.0 * log_decay)) * entry * conv.astype(F32)
+                    jnp.sqrt(one_minus_square(decay, log_decay)) * entry * conv.astype(F32)
                 )
             return carry
         lax.fori_loop(begin, end, body, 0)
@@ -361,18 +385,12 @@
         ybuf[y, :, 0:rnn] = total_a
         ybuf[y, :, rnn:] = total_b
 
-    def to_others(buf, home, n, sends, recvs, target, k, arriving):
-        slot = buf.at[wrapped(home - k, n) if arriving else home]
-        return pltpu.make_async_remote_copy(
-            src_ref=slot, dst_ref=slot, send_sem=sends.at[k], recv_sem=recvs.at[k],
-            device_id={"sp": target(k)}, device_id_type=MESH,
-        )
-
-    def y_copy(k, arriving):
-        return to_others(ybuf, y, ny, y_send, y_recv, at_y, k, arriving)
-
-    def z_copy(k, arriving):
-        return to_others(zbuf, z, nz, z_send, z_recv, at_z, k, arriving)
+    def sums_to_others(buf, home, n, sem, target):
+        for k in range(1, n):
+            pltpu.make_async_remote_copy(
+                src_ref=buf.at[home], dst_ref=buf.at[home], send_sem=sem.at[0],
+                recv_sem=sem.at[1], device_id={"sp": target(k)}, device_id_type=MESH,
+            ).start()
 
     def chained(buf, n, home):
         whole = before = (jnp.ones((1, rnn), F32), jnp.zeros((1, rnn), F32))
@@ -451,26 +469,28 @@
 
     def part_copy(n):
         return pltpu.make_async_remote_copy(
-            src_ref=psend.at[n], dst_ref=precv.at[n], send_sem=part_send.at[n],
+            src_ref=psend.at[n], dst_ref=precv.at[n], send_sem=part_send,
             recv_sem=part_recv.at[n], device_id={"tp": 1 - tp}, device_id_type=MESH,
         )
 
     def products():
         def body(n, carry):
-            weight = w[n, :, :, OUT:PACKED].reshape(features, PACKED - OUT)
+            weight = w[pl.ds(2 * n, 2), :, :, OUT:PACKED].reshape(2 * features, PACKED - OUT)
             result = lax.dot_general(
                 acts[...], weight, (((1,), (1,)), ((), ())), preferred_element_type=F32
             )
-            psend[n] = result[:half].astype(BF16)
-            part_copy(n).start()
-            own[n] = result[half:]
+            for side in (0, 1):
+                part = result[:, side * features:(side + 1) * features]
+                psend[2 * n + side] = part[:half].astype(BF16)
+                part_copy(2 * n + side).start()
+                own[2 * n + side] = part[half:]
             return carry
-        lax.fori_loop(0, nz, body, 0)
+        lax.fori_loop(0, nz // 2, body, 0)
 
     def out_copy(n):
         return pltpu.make_async_copy(
             obuf.at[n], out.at[:, pl.ds(pl.multiple_of(n * features, LANES), features)],
-            out_sem.at[n],
+            out_sem,
         )
 
     def totals():
@@ -492,77 +512,76 @@
         pieces[normed[k]] = (
             0.8, functools.partial(normalize, cuts[k], cuts[k + 1]), ("halo",)
         )
-    for k in range(2):
-        pieces[f"value{k}"] = (
-            0.8, functools.partial(project, k, k + 1), complete["value"] + normed
-        )
+    pieces["value"] = (
+        1.4, functools.partial(project, VALUE, GATE), complete["value"] + normed
+    )
     for k in range(4):
         pieces[f"gates{k}"] = (
-            0.8, functools.partial(gates, 2 * k, 2 * k + 2), ("value0", "value1", "prepare")
-        )
-    pieces["scan"] = (1.5, scan, tuple(f"gates{k}" for k in range(4)))
+            0.65, functools.partial(gates, 2 * k, 2 * k + 2), ("value", "prepare")
+        )
+    pieces["scan"] = (0.9, scan, tuple(f"gates{k}" for k in range(4)))
     pieces["row_total"] = (0.1, row_total, ("y_sums",))
     pieces["carry_in"] = (0.1, carry_in, ("z_sums",))
-    for k in range(2):
-        pieces[f"gate{k}"] = (
-            0.8, functools.partial(project, 2 + k, 3 + k), complete[f"gate{k}"] + normed
-        )
-    pieces["project_pool"] = (0.8, functools.partial(project, 4, 5), complete["pool"] + normed)
-    pieces["gelu"] = (0.4, gelu, ("gate0", "gate1"))
+    pieces["gate"] = (
+        1.4, functools.partial(project, GATE, POOL - GATE), complete["gate"] + normed
+    )
+    pieces["project_pool"] = (0.8, functools.partial(project, POOL, OUT - POOL), complete["pool"] + normed)
+    pieces["gelu"] = (0.4, gelu, ("gate",))
     pieces["pool"] = (1.4, pool, ("project_pool", "prepare"))
     pieces["finish"] = (0.3, finish, ("carry_in", "gelu"))
-    outs = sum((complete[f"out{k}"] for k in range(4)), ())
-    pieces["products"] = (2.5, products, ("finish", "pool") + outs)
+    pieces["products"] = (2.5, products, ("finish", "pool") + complete["out"])
     pieces["totals"] = (1.5, totals, ("products",))
 
-    def y_all(arriving):
-        return [y_copy(k, arriving) for k in range(1, ny)]
-
-    def z_all(arriving):
-        return [z_copy(k, arriving) for k in range(1, nz)]
-
-    def started(key, arriving):
+    def start(key):
         if key == "pair":
-            return [pair]
-        if key == "halo":
-            return [halo]
-        if key == "y_sums":
-            return y_all(arriving)
-        if key == "z_sums":
-            return z_all(arriving)
-        return [gather_copy(key, arriving)]
+            pair.start()
+        elif key == "halo":
+            halo.start()
+        elif key == "y_sums":
+            sums_to_others(ybuf, y, ny, y_sem, at_y)
+        elif key == "z_sums":
+            sums_to_others(zbuf, z, nz, z_sem, at_z)
+        else:
+            gather_copy(key).start()
+
+    def wait(group):
+        if group == "pair":
+            pair.wait_recv()
+        elif group == "halo":
+            halo.wait_recv()
+        elif group == "y_sums":
+            wait_for(ybuf.at[0:ny - 1], y_sem.at[1])
+        elif group == "z_sums":
+            wait_for(zbuf.at[0:nz - 1], z_sem.at[1])
+        else:
+            arrived(group)
 
     waited = set()
 
     def settle(keys):
         for key in keys:
-            if key in copies and key not in waited:
-                waited.add(key)
-                for copy in started(key, True):
-                    copy.wait_recv()
+            group = recvs.get(key, key)
+            if key in copies and group not in waited:
+                waited.add(group)
+                wait(group)
 
     for key in planned(copies, {k: (v[0], v[2]) for k, v in pieces.items()}):
         if key in copies:
             settle(copies[key][-1])
-            for copy in started(key, False):
-                copy.start()
+            start(key)
         else:
             settle(pieces[key][-1])
             pieces[key][1]()
     settle(copies)
 
-    for group in groups:
-        all_sent(group)
-    for key in ("pair", "halo", "y_sums", "z_sums"):
-        for copy in started(key, False):
-            copy.wait_send()
-
-    def ended(n, carry):
-        part_copy(n).wait_send()
-        out_copy(n).wait()
-        return carry
-
-    lax.fori_loop(0, nz, ended, 0)
+    for group, k in send_at.items():
+        wait_for(block_of(*group, "all"), ring_send.at[k])
+    pair.wait_send()
+    halo.wait_send()
+    wait_for(ybuf.at[0:ny - 1], y_sem.at[0])
+    wait_for(zbuf.at[0:nz - 1], z_sem.at[0])
+    wait_for(psend, part_send)
+    wait_for(obuf, out_sem)
 
 
 def shards(ny, nz, tokens, norm_gain, pool_in, gate_in, value_in, pool_mix, averaging_factor,
@@ -573,7 +592,7 @@
     rnn = log_rate.shape[0]
     lines = pool_in.shape[0]
     features = ny * lines
-    table, _ = transfers_of(ny, nz, lines)
+    sends, recvs = semaphores_of(transfers_of(ny, nz, lines)[0], ny, nz)
     dma = pltpu.SemaphoreType.DMA
     vmem = pltpu.VMEM
     scratch = [
@@ -606,12 +625,11 @@
         vmem((nz, half, features), BF16),
         vmem((nz, half, features), F32),
         vmem((nz, half, features), BF16),
-        dma((15,)),
-        dma((len({key[:3] for key in table}),)),
-        dma((len(table),)),
+        dma((18,)),
+        dma((len(set(sends.values())),)),
+        dma((len(set(recvs.values())),)),
         dma, dma, dma, dma,
-        dma((ny,)), dma((ny,)), dma((nz,)), dma((nz,)),
-        dma((nz,)), dma((nz,)), dma((nz,)),
+        dma((2,)), dma((2,)), dma, dma((nz,)), dma,
     ]
     anywhere = pl.BlockSpec(memory_space=pl.ANY)
     return pl.pallas_call(

time: 78.9 us -> 70.5 us (0.89)
  Pallas kernels: 76.5 us -> 68 us
    pallas_call x1, Pallas kernels: 76.5 us -> 68 us  [shards(): pl.pallas_call(functools.partial(kernel, ny, nz), out_shape=jax.ShapeDtyp...]
where the time goes in v3:
time: 70.5 us; the launch traced here: 70.3 us
  Pallas kernels  68 us (96%)
  local copies, waits for them, and re-layouts  2.3 us (3%)
    pallas_call x1, Pallas kernels, shards(): pl.pallas_call(functools.partial(kernel, ny, nz), out_shape=jax.ShapeDtyp...  68 us
    unnamed x1, local copies, waits for them, and re-layouts  2.3 us

profile of v3, /device:TPU:1, one launch (start us, length us, event | category | flops | bytes accessed | tf_op | source)
XLA Modules:
  0.0 70.3 jit_solution(4724729765378084576)
XLA Ops:
  0.0 68.0 %layer.1 = bf16[256,2048]{1,0:T(8,128)(2,1)} custom-call(bf16[256,2048]{1,0:T(8,128)(2,1)} %refs_0_.1, f32[1,2048]{1,0:T(1,128)} %bitcast.4, bf16[32,256]{1,0:T(8,128)(2,1)} %refs_2_.1, bf16[32,512]{1,0:T(8,128)(2,1)} %refs_3_.1, bf16[32,512]{1,0:T(8,128)(2,1)} %refs_4_.1, bf16[2,128,128]{2,1,0:T(8,128)(2,1)} %refs_5_.1, f32[1,256]{1,0:T(1,128)} %bitcast.7, ...), custom_call_target="tpu_custom_call" | custom-call | tf_op jit(solution)/shard_map/layer/pallas_call | solution.py:635
  68.0 2.3 %copy.17 = bf16[256,2048]{1,0:T(8,128)(2,1)} copy(bf16[256,2048]{1,0:T(8,128)(2,1)} %layer.1) | data formatting | bytes 2097152

commit v4 on v3

--- a/solution.py
+++ b/solution.py
@@ -37,7 +37,7 @@
     ("out", 1, OUT + 640, 128, False, None),
 )
 X_RING = 4
-LINK_RATE = 40e3
+LINK_RATE = 44e3
 HOP = 2.2
 
 
@@ -162,11 +162,11 @@
 
 def kernel(ny, nz, *refs):
     (tok_in, gain_in, pool_in, gate_in, value_in, pmix_in, avg_in, taps_in, rmix_in, imix_in,
-     lrate_in, shift_in, init_in, opool_in, ornn_in, out,
+     lrate_in, shift_in, init_in, opool_in, ornn_in, own, precv,
      w, tok, nrm, proj, aa, bb, acts, shift_t, gain, pmix, avg, taps, rmix, imix, lrate, shift,
-     init, bd, soft, ends_a, ends_b, enter, carried, ybuf, zbuf, psend, precv, own, obuf,
+     init, bd, soft, ends_a, ends_b, enter, carried, ybuf, zbuf, psend,
      local_sem, ring_send, ring_recv, pair_send, pair_recv, next_send, next_recv,
-     y_sem, z_sem, part_send, part_recv, out_sem) = refs
+     y_sem, z_sem, part_send, part_recv) = refs
     half, depth = tok_in.shape
     rows = 2 * half
     seg = rows // SEGMENTS
@@ -467,10 +467,13 @@
 
     features = ny * w.shape[2]
 
+    def columns(n):
+        return pl.ds(pl.multiple_of(n * features, LANES), features)
+
     def part_copy(n):
         return pltpu.make_async_remote_copy(
-            src_ref=psend.at[n], dst_ref=precv.at[n], send_sem=part_send,
-            recv_sem=part_recv.at[n], device_id={"tp": 1 - tp}, device_id_type=MESH,
+            src_ref=psend.at[n], dst_ref=precv.at[:, columns(n)], send_sem=part_send,
+            recv_sem=part_recv, device_id={"tp": 1 - tp}, device_id_type=MESH,
         )
 
     def products():
@@ -483,23 +486,12 @@
                 part = result[:, side * features:(side + 1) * features]
                 psend[2 * n + side] = part[:half].astype(BF16)
                 part_copy(2 * n + side).start()
-                own[2 * n + side] = part[half:]
+                own[:, columns(2 * n + side)] = part[half:]
             return carry
         lax.fori_loop(0, nz // 2, body, 0)
 
-    def out_copy(n):
-        return pltpu.make_async_copy(
-            obuf.at[n], out.at[:, pl.ds(pl.multiple_of(n * features, LANES), features)],
-            out_sem,
-        )
-
     def totals():
-        def body(n, carry):
-            part_copy(n).wait_recv()
-            obuf[n] = (own[n] + precv[n].astype(F32)).astype(BF16)
-            out_copy(n).start()
-            return carry
-        lax.fori_loop(0, nz, body, 0)
+        wait_for(precv, part_recv)
 
     copies = {"pair": (None, 0, ()), "halo": (None, 0, ("pair", "own"))}
     copies.update({"y_sums": (None, 0, ("scan",)), "z_sums": (None, 0, ("row_total",))})
@@ -530,7 +522,7 @@
     pieces["pool"] = (1.4, pool, ("project_pool", "prepare"))
     pieces["finish"] = (0.3, finish, ("carry_in", "gelu"))
     pieces["products"] = (2.5, products, ("finish", "pool") + complete["out"])
-    pieces["totals"] = (1.5, totals, ("products",))
+    pieces["totals"] = (1.0, totals, ("products",))
 
     def start(key):
         if key == "pair":
@@ -581,7 +573,6 @@
     wait_for(ybuf.at[0:ny - 1], y_sem.at[0])
     wait_for(zbuf.at[0:nz - 1], z_sem.at[0])
     wait_for(psend, part_send)
-    wait_for(obuf, out_sem)
 
 
 def shards(ny, nz, tokens, norm_gain, pool_in, gate_in, value_in, pool_mix, averaging_factor,
@@ -622,21 +613,18 @@
         vmem((ny, 1, 2 * rnn), F32),
         vmem((nz, 1, 2 * rnn), F32),
         vmem((nz, half, features), BF16),
-        vmem((nz, half, features), BF16),
-        vmem((nz, half, features), F32),
-        vmem((nz, half, features), BF16),
         dma((18,)),
         dma((len(set(sends.values())),)),
         dma((len(set(recvs.values())),)),
         dma, dma, dma, dma,
-        dma((2,)), dma((2,)), dma, dma((nz,)), dma,
+        dma((2,)), dma((2,)), dma, dma,
     ]
     anywhere = pl.BlockSpec(memory_space=pl.ANY)
-    return pl.pallas_call(
+    own, theirs = pl.pallas_call(
         functools.partial(kernel, ny, nz),
-        out_shape=jax.ShapeDtypeStruct((half, depth), BF16),
+        out_shape=(vmem((half, depth), F32), vmem((half, depth), BF16)),
         in_specs=[anywhere] * 15,
-        out_specs=anywhere,
+        out_specs=(pl.BlockSpec(memory_space=vmem),) * 2,
         scratch_shapes=scratch,
         compiler_params=pltpu.CompilerParams(
             collective_id=0, has_side_effects=True, vmem_limit_bytes=56 * 1024 * 1024
@@ -645,6 +633,7 @@
     )(tokens, norm_gain[None], pool_in, gate_in, value_in, pool_mix, averaging_factor[None],
       conv_taps, rate_mix, input_mix, log_rate[None], decay_shift, initial_state[None], out_pool,
       out_rnn)
+    return (own + theirs.astype(F32)).astype(BF16)
 
 
 def grid_of(count):

time: 70.5 us -> 66.8 us (0.948)
  Pallas kernels: 68 us -> 65.4 us
  local copies, waits for them, and re-layouts: 2.3 us -> 0 us
  other arithmetic: 0 us -> 1.26 us
    pallas_call x1, Pallas kernels: 68 us -> 65.4 us  [shards(): pl.pallas_call(functools.partial(kernel, ny, nz), out_shape=(vmem((half,...]
    unnamed x1 -> x0, local copies, waits for them, and re-layouts: 2.3 us -> none
    convert_element_type x0 -> x1, other arithmetic: none -> 1.26 us  [shards(): return (own + theirs.astype(F32)).astype(BF16)]
where the time goes in v4:
time: 66.8 us; the launch traced here: 66.7 us
  Pallas kernels  65.4 us (98%)
  other arithmetic  1.26 us (2%)
    pallas_call x1, Pallas kernels, shards(): pl.pallas_call(functools.partial(kernel, ny, nz), out_shape=(vmem((half,...  65.4 us

profile of v4, /device:TPU:1, one launch (start us, length us, event | category | flops | bytes accessed | tf_op | source)
XLA Modules:
  0.0 66.7 jit_solution(15752347800792736727)
XLA Ops:
  0.0 65.4 %layer.1 = (f32[256,2048]{1,0:T(8,128)S(1)}, bf16[256,2048]{1,0:T(8,128)(2,1)S(1)}) custom-call(bf16[256,2048]{1,0:T(8,128)(2,1)} %refs_0_.1, f32[1,2048]{1,0:T(1,128)} %bitcast.4, bf16[32,256]{1,0:T(8,128)(2,1)} %refs_2_.1, bf16[32,512]{1,0:T(8,128)(2,1)} %refs_3_.1, bf16[32,512]{1,0:T(8,128)(2,1)} %refs_4_.1, bf16[2,128,128]{2,1,0:T(8,128)(2,1)} %refs_5_.1, ...), custom_call_target="tpu_custom_call" | custom-call | tf_op jit(solution)/shard_map/layer/pallas_call | solution.py:623
  65.5 1.3 %add_convert_fusion = bf16[256,2048]{1,0:T(8,128)(2,1)} fusion(f32[256,2048]{1,0:T(8,128)S(1)} %get-tuple-element.7, bf16[256,2048]{1,0:T(8,128)(2,1)S(1)} %get-tuple-element.8), kind=kLoop, calls=%fused_computation | loop fusion | flops 1572864 | bytes 4194304 | tf_op jit(solution)/shard_map/convert_element_type | solution.py:636

commit v5 on v4

--- a/solution.py
+++ b/solution.py
@@ -38,7 +38,7 @@
 )
 X_RING = 4
 LINK_RATE = 44e3
-HOP = 2.2
+HOP = 2.6
 
 
 def transfers_of(ny, nz, lines):
@@ -181,6 +181,9 @@
     def at_z(k):
         return wrapped(z + k, nz) * ny + y
 
+    def wait_for(ref, sem):
+        pltpu.make_async_copy(ref, ref, sem).wait()
+
     def local(k, src, dst):
         return pltpu.make_async_copy(src, dst, local_sem.at[k])
 
@@ -196,13 +199,13 @@
                 cols, from_ = pl.ds(first + skip, width), pl.ds(first - base + skip, width)
             else:
                 cols, from_ = pl.ds(first, width), pl.ds(first - base, width)
-            packing.append(local(len(packing), src.at[:, from_], mine.at[:, cols]))
-    packing.append(local(len(packing), ornn_in, mine.at[:, OUT:OUT + rnn]))
-    packing.append(local(len(packing), opool_in, mine.at[:, OUT + rnn:PACKED]))
+            packing.append(local(0, src.at[:, from_], mine.at[:, cols]))
+    packing.append(local(0, ornn_in, mine.at[:, OUT:OUT + rnn]))
+    packing.append(local(0, opool_in, mine.at[:, OUT + rnn:PACKED]))
     my_rows = pl.ds(pl.multiple_of(REACH + tp * half, REACH), half)
-    own_tokens = local(8, tok_in, tok.at[my_rows])
+    own_tokens = local(1, tok_in, tok.at[my_rows])
     small = [
-        local(9 + k, src, dst)
+        local(2 + k, src, dst)
         for k, (src, dst) in enumerate(
             [(gain_in, gain), (pmix_in, pmix), (avg_in, avg), (taps_in, taps), (rmix_in, rmix),
              (imix_in, imix), (lrate_in, lrate), (shift_in, shift), (init_in, init)]
@@ -221,8 +224,8 @@
         pl.semaphore_signal(
             barrier, inc=1, device_id={"fs": wrapped(x + way, X_RING)}, device_id_type=MESH
         )
-    for copy in packing:
-        copy.wait()
+    taken = PACKED - sum(width // 2 for _, _, _, width, shared, _ in WINDOWS if shared)
+    wait_for(w.at[0, 0, :, 0:taken], local_sem.at[0])
     pl.semaphore_wait(barrier, len(peers) + 3)
 
     pair = pltpu.make_async_remote_copy(
@@ -290,9 +293,6 @@
         other = slice(None) if phase == 2 else 0
         some = slice(0, size) if what == "all" else 0
         return w.at[other, some, :, cols] if along_y else w.at[some, other, :, cols]
-
-    def wait_for(ref, sem):
-        pltpu.make_async_copy(ref, ref, sem).wait()
 
     def arrived(group):
         sem = ring_recv.at[recv_at[group]]
@@ -613,7 +613,7 @@
         vmem((ny, 1, 2 * rnn), F32),
         vmem((nz, 1, 2 * rnn), F32),
         vmem((nz, half, features), BF16),
-        dma((18,)),
+        dma((11,)),
         dma((len(set(sends.values())),)),
         dma((len(set(recvs.values())),)),
         dma, dma, dma, dma,

time: 66.8 us -> 66.7 us (level)
  no operation moved by 1% of the time
where the time goes in v5:
time: 66.7 us; the launch traced here: 66.6 us
  Pallas kernels  65.3 us (98%)
  other arithmetic  1.26 us (2%)
    pallas_call x1, Pallas kernels, shards(): pl.pallas_call(functools.partial(kernel, ny, nz), out_shape=(vmem((half,...  65.3 us

profile of v5, /device:TPU:1, one launch (start us, length us, event | category | flops | bytes accessed | tf_op | source)
XLA Modules:
  0.0 66.6 jit_solution(7208260634792561728)
XLA Ops:
  0.0 65.3 %layer.1 = (f32[256,2048]{1,0:T(8,128)S(1)}, bf16[256,2048]{1,0:T(8,128)(2,1)S(1)}) custom-call(bf16[256,2048]{1,0:T(8,128)(2,1)} %refs_0_.1, f32[1,2048]{1,0:T(1,128)} %bitcast.4, bf16[32,256]{1,0:T(8,128)(2,1)} %refs_2_.1, bf16[32,512]{1,0:T(8,128)(2,1)} %refs_3_.1, bf16[32,512]{1,0:T(8,128)(2,1)} %refs_4_.1, bf16[2,128,128]{2,1,0:T(8,128)(2,1)} %refs_5_.1, ...), custom_call_target="tpu_custom_call" | custom-call | tf_op jit(solution)/shard_map/layer/pallas_call | solution.py:623
  65.3 1.3 %add_convert_fusion = bf16[256,2048]{1,0:T(8,128)(2,1)} fusion(f32[256,2048]{1,0:T(8,128)S(1)} %get-tuple-element.7, bf16[256,2048]{1,0:T(8,128)(2,1)S(1)} %get-tuple-element.8), kind=kLoop, calls=%fused_computation | loop fusion | flops 1572864 | bytes 4194304 | tf_op jit(solution)/shard_map/convert_element_type | solution.py:636
